TPU v7x, 512 devices: a whole 4x4x16 slice. The times are simulated.
512 devices in a mesh: ep: 16 (over y, x), tp: 32 (over z, core).
Axes of the slice: x: 4, y: 4, z: 16, core: 2. Of those that a mesh axis runs over, the one named last changes fastest.
Arguments:
- tokens: bfloat16 [4096, 2048], P('ep', 'tp'), may hold values from -600 to 600
- pre_gain: float32 [2048], P('tp'), may hold values from 0.1 to 1.9
- expert_gate: bfloat16 [16, 2048, 8192], P('ep', None, 'tp'), may hold values from -0.125 to 0.125
- expert_up: bfloat16 [16, 2048, 8192], P('ep', None, 'tp'), may hold values from -0.125 to 0.125
- expert_down: bfloat16 [16, 8192, 2048], P('ep', 'tp'), may hold values from -8 to 8
- routes: int32 [4096, 2], P('ep'), may hold values from 0 to 15, all different within a row; in each aligned block of 256 rows (0 to 255, 256 to 511, ...) at most 48 rows name the same one
- route_weights: float32 [4096, 2], P('ep'), may hold values from 0.1 to 1
- post_gain: float32 [2048], P('tp'), may hold values from 0.1 to 1.9
Outputs:
- layer_out: bfloat16 [4096, 2048], P('ep', 'tp')
Inputs may be any that keep to these rules, and one draw needn't show every extreme that they name: `routes`: each token names 2 different experts. Among the 256 tokens of one index of ep no expert is named more than 48 times, a bound that some expert reaches in some of these blocks.
All inputs are finite; a program needn't handle non-finite values.
Results may differ from a plain program's by a relative error of at most 0.024.
Values may be sent and summed in bfloat16 or wider, within the bound.
No kernel may reach another device: no remote copies, remote signals or barrier semaphores. Data moves between devices by JAX's collectives and lax.ppermute only.
A program may use at most 64 MiB of HBM per device.

v0:
```python
import jax
import jax.numpy as jnp
from jax import lax
from jax.sharding import Mesh
from jax.sharding import PartitionSpec as P

TP = ("tp_0", "tp_1")


EPSILON = 1e-06


def sent_to_all(value, axis):
    copies = jnp.broadcast_to(value, (lax.axis_size(axis), *value.shape))
    return lax.all_to_all(copies, axis, split_axis=0, concat_axis=0, tiled=True)


def taken_together(value, axis):
    everything = sent_to_all(value, axis)
    return jnp.sum(everything, axis=0)


def own_block(parts, axes, turns):
    lengths = [lax.axis_size(a) for a in axes]
    parts = parts.reshape(*lengths, *parts.shape[1:])
    parts = parts.transpose(*turns, *range(len(axes), parts.ndim))
    parts = parts.reshape(-1, *parts.shape[len(axes) :])
    for k in turns:
        parts = lax.psum_scatter(parts, axes[k], scatter_dimension=0, tiled=True)
    return parts[0]


def split_up(value, dim, peers):
    before, after = (value.shape[:dim], value.shape[dim + 1 :])
    return jnp.moveaxis(value.reshape(*before, peers, -1, *after), dim, 0)


def summed_rows(value, axes, turns, dim):
    peers = lax.axis_size(axes)
    return own_block(split_up(value, dim, peers), axes, turns)


def local(tokens, pre_gain, expert_gate, expert_up, expert_down, routes, route_weights, post_gain):
    local_experts = expert_gate.shape[0]
    groups = lax.axis_size("ep")
    experts_all = local_experts * groups
    tok_rows, part_width = tokens.shape
    full_width = part_width * lax.axis_size(TP)
    capacity = 3 * tok_rows // experts_all
    values = tokens.astype(jnp.float32)
    input_sq = taken_together(jnp.sum(values * values, axis=-1), TP)
    normed = (
        values * lax.rsqrt(input_sq / full_width + EPSILON)[:, None] * pre_gain[None, :]
    ).astype(jnp.bfloat16)
    onehot = (routes[:, :, None] == jnp.arange(experts_all, dtype=jnp.int32)).astype(jnp.int32)
    onehot = onehot.reshape(tok_rows * 2, experts_all)
    earlier = jnp.cumsum(onehot, axis=0) - onehot
    slots = jnp.sum(earlier * onehot, axis=-1).reshape(tok_rows, 2)
    positions = routes * capacity + slots
    places = jnp.arange(experts_all * capacity, dtype=jnp.int32)
    first_pick = (places[:, None] == positions[None, :, 0]).astype(jnp.bfloat16)
    second_pick = (places[:, None] == positions[None, :, 1]).astype(jnp.bfloat16)
    dispatch = first_pick + second_pick
    outgoing = jnp.dot(dispatch, normed, preferred_element_type=jnp.float32).astype(jnp.bfloat16)
    arrived = lax.all_to_all(outgoing, "ep", split_axis=0, concat_axis=0, tiled=True)
    fragment = lax.all_gather(arrived, TP, axis=1, tiled=True)
    count = fragment.shape[1]
    grouped = fragment.reshape(groups, local_experts, capacity, count)
    gate_pre = jnp.einsum(
        "secw,ewf->secf", grouped, expert_gate, preferred_element_type=jnp.float32
    )
    up_pre = jnp.einsum("secw,ewf->secf", grouped, expert_up, preferred_element_type=jnp.float32)
    hidden = (jax.nn.silu(gate_pre) * up_pre).astype(jnp.bfloat16)
    product = jnp.einsum("secf,efd->dsec", hidden, expert_down, preferred_element_type=jnp.float32)
    summed = summed_rows(
        product.reshape(part_width * lax.axis_size(TP), groups * local_experts * capacity).astype(
            jnp.bfloat16
        ),
        TP,
        (1, 0),
        0,
    ).astype(jnp.float32)
    expert_out = summed.astype(jnp.bfloat16)
    returned = lax.all_to_all(expert_out, "ep", split_axis=1, concat_axis=1, tiled=True)
    contract = (((0,), (1,)), ((), ()))
    first_out = lax.dot_general(first_pick, returned, contract, preferred_element_type=jnp.float32)
    second_out = lax.dot_general(
        second_pick, returned, contract, preferred_element_type=jnp.float32
    )
    combined = route_weights[:, 0:1] * first_out + route_weights[:, 1:2] * second_out
    output_sq = taken_together(jnp.sum(combined * combined, axis=-1), TP)
    scaled = combined * lax.rsqrt(output_sq / full_width + EPSILON)[:, None] * post_gain[None, :]
    return scaled.astype(jnp.bfloat16)


def solution(mesh):
    torus = Mesh(mesh.devices.reshape(mesh.shape["ep"], 16, 2), ("ep", "tp_0", "tp_1"))
    in_specs = (
        P("ep", TP),
        P(TP),
        P("ep", None, TP),
        P("ep", None, TP),
        P("ep", TP, None),
        P("ep", None),
        P("ep", None),
        P(TP),
    )
    out_specs = P("ep", TP)
    return jax.shard_map(local, mesh=torus, in_specs=in_specs, out_specs=out_specs, check_vma=False)
```

profile of v0, /device:TPU:1, one launch (start us, length us, event | category | flops | bytes accessed | tf_op | source)
XLA Modules:
  0.0 277.1 jit_solution(4352224880434988949)
XLA Ops:
  6.5 0.0 copy-start
  6.5 0.9 fusion.16
  7.4 0.6 broadcast_in_dim.4
  8.0 16.7 %all-to-all-start = ((f32[32,1,256]{2,1,0:T(1,128)}), f32[32,1,256]{2,1,0:T(1,128)S(1)}, u32[]{:S(2)}, u32[]{:S(2)}) async-start(f32[32,1,256]{2,1,0:T(1,128)} %broadcast_in_dim.4), calls=%async_computation | async-start | bytes 65536 | tf_op jit(solution)/shard_map/all_to_all | solution.py:15
  24.8 0.0 all-gather.2.cloned.1.call-start
  24.8 0.8 copy.64
  25.7 0.1 eq.61
  25.8 0.1 eq.57
  26.0 1.2 reduce-window.6
  27.1 0.2 slice_reduce_fusion
  27.4 0.1 fusion.22
  27.5 0.1 reshape.75
  27.6 0.1 copy.67
  27.7 0.7 multiply_add_fusion
  28.4 8.4 %all-to-all-done = f32[32,1,256]{2,1,0:T(1,128)S(1)} async-done(((f32[32,1,256]{2,1,0:T(1,128)}), f32[32,1,256]{2,1,0:T(1,128)S(1)}, u32[]{:S(2)}, u32[]{:S(2)}) %all-to-all-start) | async-done | bytes 32800 | tf_op jit(solution)/shard_map/all_to_all | solution.py:15
  36.8 0.1 reduce_sum.47
  36.9 1.1 convolution_convert_fusion.1
  38.0 0.2 copy.77
  38.2 0.2 reshape.84
  38.3 13.2 %all_to_all.36 = bf16[16,2,1536]{2,1,0:T(2,128)(2,1)S(1)} all-to-all(bf16[16,2,1536]{2,1,0:T(2,128)(2,1)S(1)} %reshape.84), channel_id=1, replica_groups=mesh['ep'=16,'tp_0'=16,'tp_1'=2] {'ep'}, dimensions={0} | all-to-all | bytes 196608 | tf_op jit(solution)/shard_map/all_to_all | solution.py:65
  51.5 0.2 reshape.85
  51.7 0.8 copy.78
  52.5 0.0 all-gather.2.cloned.1.call-update
  52.5 0.0 copy-start.4
  52.5 0.0 reduce-scatter.3.cloned.1.call-start
  52.6 63.2 %all-gather.2.cloned.1.call-done = bf16[768,2048]{0,1:T(8,128)(2,1)} async-done(((bf16[768,64]{0,1:T(8,128)(2,1)}), bf16[768,2048]{0,1:T(8,128)(2,1)}) %all-gather.2.cloned.1.call-update) | async-done | bytes 3145744 | tf_op jit(solution)/shard_map/all_gather | solution.py:66
  115.7 4.7 %copy.71 = bf16[768,2048]{1,0:T(8,128)(2,1)} copy(bf16[768,2048]{0,1:T(8,128)(2,1)} %all-gather.2.cloned.1.call-done) | data formatting | bytes 6291456 | tf_op jit(solution)/shard_map/all_gather | solution.py:66
  120.4 3.0 %convolution_bitcast_fusion.1 = f32[16,1,48,256]{3,2,0,1:T(8,128)S(1)} fusion(bf16[16,48,2048]{2,1,0:T(8,128)(2,1)} %bitcast.71, bf16[1,2048,256]{2,1,0:T(8,128)(2,1)S(1)} %copy-done.4), kind=kOutput, calls=%fused_computation.3 | convolution fusion | flops 805306368 | bytes 4980736 | tf_op jit(solution)/shard_map/secw,ewf->secf/dot_general | solution.py:69
  123.5 0.1 copy-done.5
  123.6 1.0 fusion.2
  124.6 2.7 fusion
  127.3 4.6 %copy.72 = bf16[2048,768]{1,0:T(8,128)(2,1)} copy(bf16[2048,768]{0,1:T(8,128)(2,1)} %fusion) | data formatting | bytes 6291456 | tf_op jit(solution)/shard_map/convert_element_type | solution.py:76
  131.9 3.9 %copy.73 = bf16[2,16,64,768]{3,2,1,0:T(8,128)(2,1)} copy(bf16[2,16,64,768]{3,2,0,1:T(8,128)(2,1)} %bitcast.70) | data formatting | bytes 6291456 | tf_op jit(solution)/shard_map/transpose | solution.py:26
  135.8 0.0 reduce-scatter.3.cloned.1.call-update
  135.9 0.0 reduce-scatter.5.cloned.1.call-start
  135.9 18.9 %reduce-scatter.3.cloned.1.call-done = bf16[16,64,768]{2,1,0:T(8,128)(2,1)} async-done(((bf16[32,64,768]{2,1,0:T(8,128)(2,1)}), bf16[16,64,768]{2,1,0:T(8,128)(2,1)}) %reduce-scatter.3.cloned.1.call-update) | async-done | bytes 1572880 | tf_op jit(solution)/shard_map/reduce_scatter | solution.py:29
  154.8 0.0 reduce-scatter.5.cloned.1.call-update
  154.8 66.2 %reduce-scatter.5.cloned.1.call-done = bf16[1,64,768]{2,1,0:T(8,128)(2,1)} async-done(((bf16[16,64,768]{2,1,0:T(8,128)(2,1)}), bf16[1,64,768]{2,1,0:T(8,128)(2,1)}) %reduce-scatter.5.cloned.1.call-update) | async-done | bytes 98320 | tf_op jit(solution)/shard_map/reduce_scatter | solution.py:29
  221.0 1.1 copy.79
  222.1 0.8 reshape.86
  222.9 6.4 %all-to-all-start.2 = ((bf16[16,2,1536]{2,1,0:T(2,128)(2,1)}), bf16[16,2,1536]{2,1,0:T(2,128)(2,1)S(1)}, u32[]{:S(2)}, u32[]{:S(2)}) async-start(bf16[16,2,1536]{2,1,0:T(2,128)(2,1)} %reshape.86), calls=%async_computation.4 | async-start | bytes 196608 | tf_op jit(solution)/shard_map/all_to_all | solution.py:84
  229.4 6.6 %all-to-all-done.2 = bf16[16,2,1536]{2,1,0:T(2,128)(2,1)S(1)} async-done(((bf16[16,2,1536]{2,1,0:T(2,128)(2,1)}), bf16[16,2,1536]{2,1,0:T(2,128)(2,1)S(1)}, u32[]{:S(2)}, u32[]{:S(2)}) %all-to-all-start.2) | async-done | bytes 98336 | tf_op jit(solution)/shard_map/all_to_all | solution.py:84
  236.0 0.2 reshape.87
  236.2 0.3 convolution_multiply_fusion.1
  236.5 0.3 multiply_reduce_fusion
  236.8 33.0 %all_to_all.37 = f32[32,1,256]{2,1,0:T(1,128)S(1)} all-to-all(f32[32,1,256]{2,1,0:T(1,128)S(1)} %broadcast_in_dim.5), channel_id=1, replica_groups=mesh['ep'=16,'tp_0'=16,'tp_1'=2] {'tp_0','tp_1'}, dimensions={0} | all-to-all | bytes 65536 | tf_op jit(solution)/shard_map/all_to_all | solution.py:15
  269.8 0.1 reduce_sum.49
  269.9 0.7 multiply_convert_fusion
  (17 shorter events, 0.1 us)
Async XLA Ops:
  6.5 118.0 %copy-start = (bf16[1,256,2048]{2,1,0:T(8,128)(2,1)S(1)}, bf16[1,256,2048]{2,1,0:T(8,128)(2,1)}, u32[]{:S(2)}) copy-start(bf16[1,256,2048]{2,1,0:T(8,128)(2,1)} %param.12) | copy-start | bytes 3145732
  8.0 28.8 %all-to-all-start = ((f32[32,1,256]{2,1,0:T(1,128)}), f32[32,1,256]{2,1,0:T(1,128)S(1)}, u32[]{:S(2)}, u32[]{:S(2)}) async-start(f32[32,1,256]{2,1,0:T(1,128)} %broadcast_in_dim.4), calls=%async_computation | async-start | bytes 65536 | tf_op jit(solution)/shard_map/all_to_all | solution.py:15
  24.8 90.9 %all-gather.2.cloned.1.call-start = ((), (), s32[]{:S(2)}) async-start(), calls=%async_computation.6 | async-start | bytes 3244032 | tf_op jit(solution)/shard_map/all_gather | solution.py:66
  52.5 67.9 %copy-start.4 = (bf16[1,2048,256]{2,1,0:T(8,128)(2,1)S(1)}, bf16[1,2048,256]{2,1,0:T(8,128)(2,1)}, u32[]{:S(2)}) copy-start(bf16[1,2048,256]{2,1,0:T(8,128)(2,1)} %param.10) | copy-start | bytes 3145732
  52.5 102.3 %reduce-scatter.3.cloned.1.call-start = ((), (), s32[]{:S(2)}) async-start(), calls=%async_computation.7 | async-start | bytes 4718592 | tf_op jit(solution)/shard_map/reduce_scatter | solution.py:29
  120.4 3.1 %copy-start.1 = (bf16[768,2048]{1,0:T(8,128)(2,1)S(1)}, bf16[768,2048]{1,0:T(8,128)(2,1)}, u32[]{:S(2)}) copy-start(bf16[768,2048]{1,0:T(8,128)(2,1)} %copy.71) | copy-start | bytes 9437188
  120.4 3.1 %copy-start.5 = (bf16[1,2048,256]{2,1,0:T(8,128)(2,1)S(1)}, bf16[1,2048,256]{2,1,0:T(8,128)(2,1)}, u32[]{:S(2)}) copy-start(bf16[1,2048,256]{2,1,0:T(8,128)(2,1)} %param.11) | copy-start | bytes 3145732
  135.8 93.5 %copy-start.2 = (f32[256,2]{0,1:T(2,128)S(1)}, f32[256,2]{0,1:T(2,128)}, u32[]{:S(2)}) copy-start(f32[256,2]{0,1:T(2,128)} %param.14) | copy-start | bytes 6148
  135.8 134.0 %copy-start.3 = (f32[64]{0:T(128)S(1)}, f32[64]{0:T(128)}, u32[]{:S(2)}) copy-start(f32[64]{0:T(128)} %param.15) | copy-start | bytes 772
  135.9 85.2 %reduce-scatter.5.cloned.1.call-start = ((), (), s32[]{:S(2)}) async-start(), calls=%async_computation.8 | async-start | bytes 1671168 | tf_op jit(solution)/shard_map/reduce_scatter | solution.py:29
  222.9 13.1 %all-to-all-start.2 = ((bf16[16,2,1536]{2,1,0:T(2,128)(2,1)}), bf16[16,2,1536]{2,1,0:T(2,128)(2,1)S(1)}, u32[]{:S(2)}, u32[]{:S(2)}) async-start(bf16[16,2,1536]{2,1,0:T(2,128)(2,1)} %reshape.86), calls=%async_computation.4 | async-start | bytes 196608 | tf_op jit(solution)/shard_map/all_to_all | solution.py:84
Sparse Core Ops, SparseCore 0:
  52.6 63.0 all-gather.1
  136.0 18.7 reduce-scatter.2
  157.6 63.3 reduce-scatter.4
where the time goes:
time: 278 us; the launch traced here: 277 us
  waiting for transfers between devices  163 us (59%)
  blocking collectives  46.2 us (17%)
  starting transfers between devices  23.3 us (8%)
  local copies, waits for them, and re-layouts  18.8 us (7%)
  between operations  13.3 us (5%)
  matrix products  8.38 us (3%)
  other arithmetic  3.68 us (1%)
    reduce_scatter x2, waiting for transfers between devices, own_block(): parts = lax.psum_scatter(parts, axes[k], scatter_dimension=0, tiled=True)  85.1 us
    all_gather x1, waiting for transfers between devices, local(): fragment = lax.all_gather(arrived, TP, axis=1, tiled=True)  63.2 us
    all_to_all x1, blocking collectives, sent_to_all(): return lax.all_to_all(copies, axis, split_axis=0, concat_axis=0, tiled=True)  33 us
    all_to_all x1, starting transfers between devices, sent_to_all(): return lax.all_to_all(copies, axis, split_axis=0, concat_axis=0, tiled=True)  16.7 us
    all_to_all x1, blocking collectives, local(): lax.all_to_all(outgoing, 'ep', split_axis=0, concat_axis=0, tiled=True)  13.2 us
    all_to_all x1, waiting for transfers between devices, sent_to_all(): return lax.all_to_all(copies, axis, split_axis=0, concat_axis=0, tiled=True)  8.44 us
    all_to_all x1, waiting for transfers between devices, local(): lax.all_to_all(expert_out, 'ep', split_axis=1, concat_axis=1, tiled=True)  6.64 us
    all_to_all x1, starting transfers between devices, local(): lax.all_to_all(expert_out, 'ep', split_axis=1, concat_axis=1, tiled=True)  6.45 us
  transfers between devices with their start and end apart: 5, of which 5 were waited for; matrix products, arithmetic and copies ran while one was open for 1% of the time, Pallas kernels for 0%

commit v1 on v0

v1 whole, which is shorter than its diff:
```python
import jax
import jax.numpy as jnp
from jax import lax
from jax.experimental import pallas as pl
from jax.experimental.pallas import tpu as pltpu
from jax.sharding import Mesh
from jax.sharding import PartitionSpec as P

TP = ("tp_0", "tp_1")
EPSILON = 1e-06
F32 = jnp.float32
BF16 = jnp.bfloat16


def sent_to_all(value, axis):
    copies = jnp.broadcast_to(value, (lax.axis_size(axis), *value.shape))
    return lax.all_to_all(copies, axis, split_axis=0, concat_axis=0, tiled=True)


def swapped(value):
    return lax.ppermute(value, "tp_1", [(0, 1), (1, 0)])


def three_pieces(value):
    high = lax.reduce_precision(value, 8, 7)
    middle = lax.reduce_precision(value - high, 8, 7)
    low = lax.reduce_precision(value - high - middle, 8, 7)
    return jnp.stack([high, middle, low]).astype(BF16)


def expert_kernel(core, own, peer, gate, up, down, keep, send, split_down):
    mine = core[0]
    other = 1 - mine
    half = own.shape[1]
    hidden_units = gate.shape[-1]
    row = lax.broadcasted_iota(jnp.int32, (256, 256), 0)
    col = lax.broadcasted_iota(jnp.int32, (256, 256), 1)
    source = ((col // 64) % 2) * 128 + (col // 128) * 64 + col % 64
    shuffle = (row == source).astype(F32).astype(BF16)
    for block in range(down.shape[1] // 256):
        turned = jnp.dot(
            down[:, block * 256 : block * 256 + 256], shuffle, preferred_element_type=F32
        ).astype(BF16)
        for side in range(2):
            split_down[side, :, block * 128 : block * 128 + 128] = turned[
                :, side * 128 : side * 128 + 128
            ]
    gate_own = gate[:, mine].reshape(half, hidden_units)
    gate_peer = gate[:, other].reshape(half, hidden_units)
    up_own = up[:, mine].reshape(half, hidden_units)
    up_peer = up[:, other].reshape(half, hidden_units)
    down_own = split_down[mine]
    down_peer = split_down[other]
    step = 256
    for start in range(0, own.shape[0], step):
        here = slice(start, start + step)
        a, b = own[here, :], peer[here, :]
        gate_pre = jnp.dot(a, gate_own, preferred_element_type=F32) + jnp.dot(
            b, gate_peer, preferred_element_type=F32
        )
        up_pre = jnp.dot(a, up_own, preferred_element_type=F32) + jnp.dot(
            b, up_peer, preferred_element_type=F32
        )
        hidden = (gate_pre / (1.0 + jnp.exp(-gate_pre)) * up_pre).astype(BF16)
        send[here, :] = jnp.dot(hidden, down_peer, preferred_element_type=F32).astype(BF16)
        keep[here, :] = jnp.dot(hidden, down_own, preferred_element_type=F32).astype(BF16)


def local(tokens, pre_gain, expert_gate, expert_up, expert_down, routes, route_weights, post_gain):
    groups = lax.axis_size("ep")
    columns = lax.axis_size("tp_0")
    tok_rows, part_width = tokens.shape
    full_width = part_width * lax.axis_size(TP)
    half_width = part_width * columns
    capacity = 3 * tok_rows // groups
    slots_all = groups * capacity
    core = lax.axis_index("tp_1").astype(jnp.int32)

    values = tokens.T.astype(F32)
    partial_sq = jnp.sum(values * values, axis=0)
    scaled = (values * pre_gain[:, None]).astype(BF16)
    pieces = jnp.pad(three_pieces(partial_sq), ((0, 5), (0, 0)))
    payload = jnp.concatenate([scaled, pieces], axis=0)
    gathered = lax.all_gather(payload, "tp_0", axis=0, tiled=False)
    half_sq = jnp.sum(gathered[:, part_width : part_width + 3].astype(F32), axis=(0, 1))
    input_sq = half_sq + swapped(half_sq[None])[0]
    row_scale = lax.rsqrt(input_sq / full_width + EPSILON)
    normed = (
        (gathered[:, :part_width].astype(F32) * row_scale).astype(BF16).reshape(half_width, tok_rows)
    )

    chosen = routes.T
    experts = lax.broadcasted_iota(jnp.int32, (groups, tok_rows), 0)
    first_hot = (experts == chosen[0]).astype(F32)
    second_hot = (experts == chosen[1]).astype(F32)
    before = (
        lax.broadcasted_iota(jnp.int32, (tok_rows, tok_rows), 0)
        < lax.broadcasted_iota(jnp.int32, (tok_rows, tok_rows), 1)
    ).astype(BF16)
    earlier = jnp.dot(
        (first_hot + second_hot).astype(BF16), before, preferred_element_type=F32
    )
    first_slot = jnp.sum(earlier * first_hot, axis=0).astype(jnp.int32)
    second_slot = jnp.sum(earlier * second_hot, axis=0).astype(jnp.int32)
    places = lax.broadcasted_iota(jnp.int32, (slots_all, tok_rows), 0)
    first_pick = (places == chosen[0] * capacity + first_slot).astype(BF16)
    second_pick = (places == chosen[1] * capacity + second_slot).astype(BF16)

    outgoing = lax.dot_general(
        first_pick + second_pick, normed, (((1,), (1,)), ((), ())), preferred_element_type=F32
    ).astype(BF16)
    own = lax.all_to_all(
        outgoing.reshape(groups, capacity, half_width), "ep", split_axis=0, concat_axis=0, tiled=True
    ).reshape(slots_all, half_width)
    peer = swapped(own)

    vmem = pl.BlockSpec(memory_space=pltpu.VMEM)
    units = expert_gate.shape[-1]
    keep, send = pl.pallas_call(
        expert_kernel,
        in_specs=[pl.BlockSpec(memory_space=pltpu.SMEM), vmem, vmem, vmem, vmem, vmem],
        out_specs=[vmem, vmem],
        out_shape=[jax.ShapeDtypeStruct((slots_all, half_width), BF16)] * 2,
        scratch_shapes=[pltpu.VMEM((2, units, half_width), BF16)],
        compiler_params=pltpu.CompilerParams(vmem_limit_bytes=48 * 1024 * 1024),
        name="expert",
    )(
        core[None],
        own,
        peer,
        expert_gate.reshape(columns, 2, part_width, units),
        expert_up.reshape(columns, 2, part_width, units),
        expert_down.reshape(units, full_width),
    )
    expert_out = (keep.astype(F32) + swapped(send).astype(F32)).astype(BF16)
    returned = lax.all_to_all(
        expert_out.reshape(groups, capacity, half_width), "ep", split_axis=0, concat_axis=0, tiled=True
    ).reshape(slots_all, half_width)

    contract = (((0,), (0,)), ((), ()))
    first_out = lax.dot_general(returned, first_pick, contract, preferred_element_type=F32)
    second_out = lax.dot_general(returned, second_pick, contract, preferred_element_type=F32)
    weights = route_weights.T
    partial = (weights[0] * first_out + weights[1] * second_out).astype(BF16)
    parts = lax.all_to_all(
        partial.reshape(columns, part_width, tok_rows), "tp_0", split_axis=0, concat_axis=0, tiled=True
    )
    combined = jnp.sum(parts.astype(F32), axis=0)
    output_sq = jnp.sum(sent_to_all(jnp.sum(combined * combined, axis=0)[None], TP), axis=(0, 1))
    result = combined * lax.rsqrt(output_sq / full_width + EPSILON) * post_gain[:, None]
    return result.astype(BF16).T


def solution(mesh):
    torus = Mesh(mesh.devices.reshape(mesh.shape["ep"], 16, 2), ("ep", "tp_0", "tp_1"))
    in_specs = (
        P("ep", TP),
        P(TP),
        P("ep", None, TP),
        P("ep", None, TP),
        P("ep", TP, None),
        P("ep", None),
        P("ep", None),
        P(TP),
    )
    out_specs = P("ep", TP)
    return jax.shard_map(local, mesh=torus, in_specs=in_specs, out_specs=out_specs, check_vma=False)
```

time: 278 us -> 181 us (0.65)
  waiting for transfers between devices: 163 us -> 31.6 us
  blocking collectives: 46.2 us -> 116 us
  local copies, waits for them, and re-layouts: 18.8 us -> 0.82 us
  between operations: 13.3 us -> 0.18 us
  matrix products: 8.38 us -> 2.14 us
  Pallas kernels: 0 us -> 6.08 us
  starting transfers between devices: 23.3 us -> 19.6 us
    reduce_scatter x2 -> x0, waiting for transfers between devices: 85.1 us -> none  [own_block(): parts = lax.psum_scatter(parts, axes[k], scatter_dimension=0, tiled=True)]
    all_gather x1 -> x0, waiting for transfers between devices: 63.2 us -> none  [local(): fragment = lax.all_gather(arrived, TP, axis=1, tiled=True)]
    all_to_all x1 -> x2, blocking collectives: 13.2 us -> 58.3 us  [the longest x1 29.3 us: local(): lax.all_to_all(outgoing.reshape(groups, capacity, half_width), 'ep', spli...]
    all_gather x0 -> x1, blocking collectives: none -> 32.1 us  [local(): gathered = lax.all_gather(payload, 'tp_0', axis=0, tiled=False)]
    all_to_all x2 -> x1, starting transfers between devices: 23.2 us -> 3.84 us  [local(): lax.all_to_all(expert_out.reshape(groups, capacity, half_width), 'ep', sp...]
    ppermute x0 -> x3, starting transfers between devices: none -> 15.8 us  [swapped(): return lax.ppermute(value, 'tp_1', [(0, 1), (1, 0)])]
    all_to_all x2 -> x1, waiting for transfers between devices: 15.1 us -> 25 us  [local(): lax.all_to_all(expert_out.reshape(groups, capacity, half_width), 'ep', sp...]
    all_to_all x1, blocking collectives: 33 us -> 25.2 us  [sent_to_all(): return lax.all_to_all(copies, axis, split_axis=0, concat_axis=0, tiled=True)]
  transfers between devices with their start and end apart: 5 -> 4, of which waited for: 5 -> 3; matrix products, arithmetic and copies ran while one was open for 1% -> 1% of each run, Pallas kernels for 0% -> 0%
where the time goes in v1:
time: 181 us; the launch traced here: 180 us
  blocking collectives  116 us (64%)
  waiting for transfers between devices  31.6 us (17%)
  starting transfers between devices  19.6 us (11%)
  Pallas kernels  6.08 us (3%)
  other arithmetic  4.51 us (2%)
  matrix products  2.14 us (1%)
    all_gather x1, blocking collectives, local(): gathered = lax.all_gather(payload, 'tp_0', axis=0, tiled=False)  32.1 us
    all_to_all x1, blocking collectives, local(): lax.all_to_all(outgoing.reshape(groups, capacity, half_width), 'ep', spli...  29.3 us
    all_to_all x1, blocking collectives, local(): lax.all_to_all(partial.reshape(columns, part_width, tok_rows), 'tp_0', sp...  29 us
    all_to_all x1, blocking collectives, sent_to_all(): return lax.all_to_all(copies, axis, split_axis=0, concat_axis=0, tiled=True)  25.2 us
    all_to_all x1, waiting for transfers between devices, local(): lax.all_to_all(expert_out.reshape(groups, capacity, half_width), 'ep', sp...  25 us
    ppermute x3, starting transfers between devices, swapped(): return lax.ppermute(value, 'tp_1', [(0, 1), (1, 0)])  15.8 us
    ppermute x3, waiting for transfers between devices, swapped(): return lax.ppermute(value, 'tp_1', [(0, 1), (1, 0)])  6.58 us
    pallas_call x1, Pallas kernels, local(): pl.pallas_call(expert_kernel, in_specs=[pl.BlockSpec(memory_space=pltpu.S...  6.08 us
  transfers between devices with their start and end apart: 4, of which 3 were waited for; matrix products, arithmetic and copies ran while one was open for 1% of the time, Pallas kernels for 0%

profile of v1, /device:TPU:1, one launch (start us, length us, event | category | flops | bytes accessed | tf_op | source)
XLA Modules:
  0.0 180.5 jit_solution(15683489545562338437)
XLA Ops:
  0.0 0.8 fusion.15
  0.9 32.1 %all-gather = bf16[1152,256]{1,0:T(8,128)(2,1)S(1)} all-gather(bf16[72,256]{1,0:T(8,128)(2,1)S(1)} %pad_maximum_fusion), channel_id=2, replica_groups=mesh['ep'=16,'tp_0'=16,'tp_1'=2] {'tp_0'}, dimensions={0}, use_global_device_ids=true | all-gather | bytes 626688 | tf_op jit(solution)/shard_map/all_gather | solution.py:84
  33.0 10.1 %collective-permute-start = (f32[1,256]{1,0:T(1,128)S(1)}, f32[1,256]{1,0:T(1,128)S(1)}, u32[]{:S(2)}, u32[]{:S(2)}) collective-permute-start(f32[1,256]{1,0:T(1,128)S(1)} %bitcast.48), channel_id=1, source_target_pairs={{0,1},{1,0},{2,3},{3,2},{4,5},{5,4},{6,7},{7,6},{8,9},{9,8},{10,11... | collective-permute-start | bytes 3080 | tf_op jit(solution)/shard_map/ppermute | solution.py:21
  43.2 0.8 fusion.26
  44.0 0.2 select_reduce_fusion.1
  44.2 0.8 multiply_add_fusion.1
  44.9 0.0 collective-permute-done
  44.9 0.1 multiply_convert_fusion
  45.1 0.6 convolution_convert_fusion
  45.7 0.0 copy-start
  45.7 0.0 copy-start.1
  45.7 0.0 copy-start.2
  45.7 29.3 %all_to_all.20 = bf16[16,48,1024]{2,1,0:T(8,128)(2,1)} all-to-all(bf16[16,48,1024]{2,1,0:T(8,128)(2,1)S(1)} %bitcast.34), channel_id=1, replica_groups=mesh['ep'=16,'tp_0'=16,'tp_1'=2] {'ep'}, dimensions={0} | all-to-all | bytes 3145728 | tf_op jit(solution)/shard_map/all_to_all | solution.py:112
  75.0 3.3 %collective-permute-start.1 = (bf16[768,1024]{1,0:T(8,128)(2,1)}, bf16[768,1024]{1,0:T(8,128)(2,1)}, u32[]{:S(2)}, u32[]{:S(2)}) collective-permute-start(bf16[768,1024]{1,0:T(8,128)(2,1)} %bitcast.17.own), channel_id=1, source_target_pairs={{0,1},{1,0},{2,3},{3,2},{4,5},{5,4},{6,7},{7,6},{8,9},{9,8},{10,11... | collective-permute-start | bytes 4718600 | tf_op jit(solution)/shard_map/ppermute | solution.py:21
  78.4 3.4 %collective-permute-done.1.peer = bf16[768,1024]{1,0:T(8,128)(2,1)} collective-permute-done((bf16[768,1024]{1,0:T(8,128)(2,1)}, bf16[768,1024]{1,0:T(8,128)(2,1)}, u32[]{:S(2)}, u32[]{:S(2)}) %collective-permute-start.1) | collective-permute-done | bytes 1572896 | tf_op jit(solution)/shard_map/ppermute | solution.py:21
  81.7 0.0 copy-done
  81.7 0.0 copy-done.1
  81.7 0.0 copy-done.2
  81.7 6.1 %expert.1 = (bf16[768,1024]{1,0:T(8,128)(2,1)S(1)}, bf16[768,1024]{1,0:T(8,128)(2,1)}) custom-call(s32[1]{0:T(128)} %bitcast.2.core, bf16[768,1024]{1,0:T(8,128)(2,1)} %bitcast.17.own, bf16[768,1024]{1,0:T(8,128)(2,1)} %collective-permute-done.1.peer, bf16[16,2,64,256]{3,2,1,0:T(8,128)(2,1)S(1)} %bitcast.31, bf16[16,2,64,256]{3,2,1,0:T(8,128)(2,1)S(1)} %bitcast.32, ...), custom_call_target="tpu_custom_call" | custom-call | tf_op jit(solution)/shard_map/expert/pallas_call | solution.py:119
  87.8 2.3 %collective-permute-start.2 = (bf16[768,1024]{1,0:T(8,128)(2,1)}, bf16[768,1024]{1,0:T(8,128)(2,1)S(1)}, u32[]{:S(2)}, u32[]{:S(2)}) collective-permute-start(bf16[768,1024]{1,0:T(8,128)(2,1)} %get-tuple-element.8), channel_id=1, source_target_pairs={{0,1},{1,0},{2,3},{3,2},{4,5},{5,4},{6,7},{7,6},{8,9},{9,8},{10,11... | collective-permute-start | bytes 4718600 | tf_op jit(solution)/shard_map/ppermute | solution.py:21
  90.1 3.2 %collective-permute-done.2 = bf16[768,1024]{1,0:T(8,128)(2,1)S(1)} collective-permute-done((bf16[768,1024]{1,0:T(8,128)(2,1)}, bf16[768,1024]{1,0:T(8,128)(2,1)S(1)}, u32[]{:S(2)}, u32[]{:S(2)}) %collective-permute-start.2) | collective-permute-done | bytes 1572896 | tf_op jit(solution)/shard_map/ppermute | solution.py:21
  93.3 1.8 %add_convert_fusion = bf16[768,1024]{1,0:T(8,128)(2,1)} fusion(bf16[768,1024]{1,0:T(8,128)(2,1)S(1)} %collective-permute-done.2, bf16[768,1024]{1,0:T(8,128)(2,1)S(1)} %get-tuple-element.7), kind=kLoop, calls=%fused_computation | loop fusion | flops 3145728 | bytes 4718592 | tf_op jit(solution)/shard_map/convert_element_type | solution.py:135
  95.2 0.0 copy-start.3
  95.2 3.8 %all-to-all-start.1 = ((bf16[16,48,1024]{2,1,0:T(8,128)(2,1)}), bf16[16,48,1024]{2,1,0:T(8,128)(2,1)S(1)}, u32[]{:S(2)}, u32[]{:S(2)}) async-start(bf16[16,48,1024]{2,1,0:T(8,128)(2,1)} %bitcast.21), calls=%async_computation.1 | async-start | bytes 3145728 | tf_op jit(solution)/shard_map/all_to_all | solution.py:136
  99.0 0.0 copy-done.3
  99.0 25.0 %all-to-all-done.1 = bf16[16,48,1024]{2,1,0:T(8,128)(2,1)S(1)} async-done(((bf16[16,48,1024]{2,1,0:T(8,128)(2,1)}), bf16[16,48,1024]{2,1,0:T(8,128)(2,1)S(1)}, u32[]{:S(2)}, u32[]{:S(2)}) %all-to-all-start.1) | async-done | bytes 1572896 | tf_op jit(solution)/shard_map/all_to_all | solution.py:136
  124.0 0.7 convolution_multiply_fusion.1
  124.7 0.7 fusion.1
  125.4 0.0 copy-start.4
  125.4 29.0 %all_to_all.21 = bf16[16,64,256]{2,1,0:T(8,128)(2,1)S(1)} all-to-all(bf16[16,64,256]{2,1,0:T(8,128)(2,1)S(1)} %bitcast.40), channel_id=1, replica_groups=mesh['ep'=16,'tp_0'=16,'tp_1'=2] {'tp_0'}, dimensions={0} | all-to-all | bytes 1048576 | tf_op jit(solution)/shard_map/all_to_all | solution.py:145
  154.4 0.1 convert_reduce_fusion
  154.5 25.2 %all_to_all.22 = f32[32,1,256]{2,1,0:T(1,128)S(1)} all-to-all(f32[32,1,256]{2,1,0:T(1,128)S(1)} %broadcast_in_dim.8), channel_id=1, replica_groups=mesh['ep'=16,'tp_0'=16,'tp_1'=2] {'tp_0','tp_1'}, dimensions={0} | all-to-all | bytes 65536 | tf_op jit(solution)/shard_map/all_to_all | solution.py:17
  179.7 0.1 reduce_sum.72
  179.8 0.0 copy-done.4
  179.8 0.7 fusion.14
  (11 shorter events, 0.1 us)
Async XLA Ops:
  33.0 11.9 %collective-permute-start = (f32[1,256]{1,0:T(1,128)S(1)}, f32[1,256]{1,0:T(1,128)S(1)}, u32[]{:S(2)}, u32[]{:S(2)}) collective-permute-start(f32[1,256]{1,0:T(1,128)S(1)} %bitcast.48), channel_id=1, source_target_pairs={{0,1},{1,0},{2,3},{3,2},{4,5},{5,4},{6,7},{7,6},{8,9},{9,8},{10,11... | collective-permute-start | bytes 3080 | tf_op jit(solution)/shard_map/ppermute | solution.py:21
  45.7 36.0 %copy-start = (bf16[1,2048,256]{2,1,0:T(8,128)(2,1)S(1)}, bf16[1,2048,256]{2,1,0:T(8,128)(2,1)}, u32[]{:S(2)}) copy-start(bf16[1,2048,256]{2,1,0:T(8,128)(2,1)} %param.10) | copy-start | bytes 3145732
  45.7 36.0 %copy-start.1 = (bf16[1,2048,256]{2,1,0:T(8,128)(2,1)S(1)}, bf16[1,2048,256]{2,1,0:T(8,128)(2,1)}, u32[]{:S(2)}) copy-start(bf16[1,2048,256]{2,1,0:T(8,128)(2,1)} %param.11) | copy-start | bytes 3145732
  45.7 36.0 %copy-start.2 = (bf16[1,256,2048]{2,1,0:T(8,128)(2,1)S(1)}, bf16[1,256,2048]{2,1,0:T(8,128)(2,1)}, u32[]{:S(2)}) copy-start(bf16[1,256,2048]{2,1,0:T(8,128)(2,1)} %param.12) | copy-start | bytes 3145732
  75.0 6.7 %collective-permute-start.1 = (bf16[768,1024]{1,0:T(8,128)(2,1)}, bf16[768,1024]{1,0:T(8,128)(2,1)}, u32[]{:S(2)}, u32[]{:S(2)}) collective-permute-start(bf16[768,1024]{1,0:T(8,128)(2,1)} %bitcast.17.own), channel_id=1, source_target_pairs={{0,1},{1,0},{2,3},{3,2},{4,5},{5,4},{6,7},{7,6},{8,9},{9,8},{10,11... | collective-permute-start | bytes 4718600 | tf_op jit(solution)/shard_map/ppermute | solution.py:21
  87.8 5.5 %collective-permute-start.2 = (bf16[768,1024]{1,0:T(8,128)(2,1)}, bf16[768,1024]{1,0:T(8,128)(2,1)S(1)}, u32[]{:S(2)}, u32[]{:S(2)}) collective-permute-start(bf16[768,1024]{1,0:T(8,128)(2,1)} %get-tuple-element.8), channel_id=1, source_target_pairs={{0,1},{1,0},{2,3},{3,2},{4,5},{5,4},{6,7},{7,6},{8,9},{9,8},{10,11... | collective-permute-start | bytes 4718600 | tf_op jit(solution)/shard_map/ppermute | solution.py:21
  95.2 3.9 %copy-start.3 = (f32[256,2]{0,1:T(2,128)S(1)}, f32[256,2]{0,1:T(2,128)}, u32[]{:S(2)}) copy-start(f32[256,2]{0,1:T(2,128)} %param.14) | copy-start | bytes 6148
  95.2 28.8 %all-to-all-start.1 = ((bf16[16,48,1024]{2,1,0:T(8,128)(2,1)}), bf16[16,48,1024]{2,1,0:T(8,128)(2,1)S(1)}, u32[]{:S(2)}, u32[]{:S(2)}) async-start(bf16[16,48,1024]{2,1,0:T(8,128)(2,1)} %bitcast.21), calls=%async_computation.1 | async-start | bytes 3145728 | tf_op jit(solution)/shard_map/all_to_all | solution.py:136
  125.4 54.4 %copy-start.4 = (f32[64]{0:T(128)S(1)}, f32[64]{0:T(128)}, u32[]{:S(2)}) copy-start(f32[64]{0:T(128)} %param.15) | copy-start | bytes 772

commit v2 on v1

v2 whole, which is shorter than its diff:
```python
import jax
import jax.numpy as jnp
from jax import lax
from jax.experimental import pallas as pl
from jax.experimental.pallas import tpu as pltpu
from jax.sharding import Mesh
from jax.sharding import PartitionSpec as P

Z = ("z8", "zp")
TP = ("z8", "zp", "tp_1")
EPSILON = 1e-06
F32 = jnp.float32
BF16 = jnp.bfloat16
STEP = 384
MIB = 1024 * 1024


def sent_to_all(value, axis):
    copies = jnp.broadcast_to(value, (lax.axis_size(axis), *value.shape))
    return lax.all_to_all(copies, axis, split_axis=0, concat_axis=0, tiled=True)


def swapped(value):
    return lax.ppermute(value, "tp_1", [(0, 1), (1, 0)])


def three_pieces(value):
    high = lax.reduce_precision(value, 8, 7)
    middle = lax.reduce_precision(value - high, 8, 7)
    low = lax.reduce_precision(value - high - middle, 8, 7)
    return jnp.stack([high, middle, low]).astype(BF16)


def own_half_kernel(core, own, gate, up, down, gate_pre, up_pre, split_down):
    mine = core[0]
    half = own.shape[1]
    hidden_units = gate.shape[-1]
    gate_own = gate[:, mine].reshape(half, hidden_units)
    up_own = up[:, mine].reshape(half, hidden_units)
    for start in range(0, own.shape[0], STEP):
        here = slice(start, start + STEP)
        rows = own[here, :]
        gate_pre[here, :] = jnp.dot(rows, gate_own, preferred_element_type=F32)
        up_pre[here, :] = jnp.dot(rows, up_own, preferred_element_type=F32)
    size = 512
    row = lax.broadcasted_iota(jnp.int32, (size, size), 0)
    col = lax.broadcasted_iota(jnp.int32, (size, size), 1)
    part = col // 64
    source = (part % 2) * 256 + ((part // 2) % 2) * 128 + (part // 4) * 64 + col % 64
    shuffle = (row == source).astype(F32).astype(BF16)
    for block in range(down.shape[1] // size):
        turned = jnp.dot(
            down[:, block * size : (block + 1) * size], shuffle, preferred_element_type=F32
        ).astype(BF16)
        for side in range(2):
            for pair in range(2):
                split_down[side, pair, :, block * 128 : block * 128 + 128] = turned[
                    :, side * 256 + pair * 128 : side * 256 + pair * 128 + 128
                ]


def peer_half_kernel(core, peer, gate_own, up_own, gate, up, split_down, hidden, send):
    other = 1 - core[0]
    half = peer.shape[1]
    hidden_units = gate.shape[-1]
    gate_peer = gate[:, other].reshape(half, hidden_units)
    up_peer = up[:, other].reshape(half, hidden_units)
    capacity = send.shape[2]
    for start in range(0, peer.shape[0], STEP):
        here = slice(start, start + STEP)
        there = slice(start // capacity, (start + STEP) // capacity)
        rows = peer[here, :]
        gate_pre = gate_own[here, :] + jnp.dot(rows, gate_peer, preferred_element_type=F32)
        up_pre = up_own[here, :] + jnp.dot(rows, up_peer, preferred_element_type=F32)
        value = (gate_pre / (1.0 + jnp.exp(-gate_pre)) * up_pre).astype(BF16)
        hidden[here, :] = value
        for pair in range(2):
            part = jnp.dot(value, split_down[other, pair], preferred_element_type=F32)
            send[there, pair] = part.astype(BF16).reshape(STEP // capacity, capacity, -1)


def keep_kernel(core, hidden, split_down, keep):
    mine = core[0]
    capacity = keep.shape[2]
    for start in range(0, hidden.shape[0], STEP):
        there = slice(start // capacity, (start + STEP) // capacity)
        value = hidden[start : start + STEP, :]
        for pair in range(2):
            part = jnp.dot(value, split_down[mine, pair], preferred_element_type=F32)
            keep[there, pair] = part.astype(BF16).reshape(STEP // capacity, capacity, -1)


def local(tokens, pre_gain, expert_gate, expert_up, expert_down, routes, route_weights, post_gain):
    groups = lax.axis_size("ep")
    columns = lax.axis_size(Z)
    pairs = lax.axis_size("zp")
    tok_rows, part_width = tokens.shape
    full_width = part_width * lax.axis_size(TP)
    half_width = part_width * columns
    capacity = 3 * tok_rows // groups
    slots_all = groups * capacity
    core = lax.axis_index("tp_1").astype(jnp.int32)

    values = tokens.T.astype(F32)
    partial_sq = jnp.sum(values * values, axis=0)
    scaled = (values * pre_gain[:, None]).astype(BF16)
    pieces = jnp.pad(three_pieces(partial_sq), ((0, 5), (0, 0)))
    payload = jnp.concatenate([scaled, pieces], axis=0)
    gathered = lax.all_gather(payload, Z, axis=0, tiled=False)
    half_sq = jnp.sum(gathered[:, part_width : part_width + 3].astype(F32), axis=(0, 1))
    input_sq = half_sq + swapped(half_sq[None])[0]
    row_scale = lax.rsqrt(input_sq / full_width + EPSILON)
    normed = (
        (gathered[:, :part_width].astype(F32) * row_scale).astype(BF16).reshape(half_width, tok_rows)
    )

    chosen = routes.T
    experts = lax.broadcasted_iota(jnp.int32, (groups, tok_rows), 0)
    first_hot = (experts == chosen[0]).astype(F32)
    second_hot = (experts == chosen[1]).astype(F32)
    before = (
        lax.broadcasted_iota(jnp.int32, (tok_rows, tok_rows), 0)
        < lax.broadcasted_iota(jnp.int32, (tok_rows, tok_rows), 1)
    ).astype(BF16)
    earlier = jnp.dot(
        (first_hot + second_hot).astype(BF16), before, preferred_element_type=F32
    )
    first_slot = jnp.sum(earlier * first_hot, axis=0).astype(jnp.int32)
    second_slot = jnp.sum(earlier * second_hot, axis=0).astype(jnp.int32)
    places = lax.broadcasted_iota(jnp.int32, (slots_all, tok_rows), 0)
    first_place = chosen[0] * capacity + first_slot
    second_place = chosen[1] * capacity + second_slot
    first_pick = (places == first_place).astype(BF16)
    second_pick = (places == second_place).astype(BF16)

    outgoing = lax.dot_general(
        first_pick + second_pick, normed, (((1,), (1,)), ((), ())), preferred_element_type=F32
    ).astype(BF16)
    own = lax.all_to_all(
        outgoing.reshape(groups, capacity, half_width), "ep", split_axis=0, concat_axis=0, tiled=True
    ).reshape(slots_all, half_width)
    peer = swapped(own)

    vmem = pl.BlockSpec(memory_space=pltpu.VMEM)
    smem = pl.BlockSpec(memory_space=pltpu.SMEM)
    units = expert_gate.shape[-1]
    width = half_width // pairs
    index = core[None]
    gate = expert_gate.reshape(columns, 2, part_width, units)
    up = expert_up.reshape(columns, 2, part_width, units)
    sent = jax.ShapeDtypeStruct((groups, pairs, capacity, width), BF16)

    def kernel(body, out_shape, *operands):
        return pl.pallas_call(
            body,
            in_specs=[smem] + [vmem] * len(operands),
            out_specs=jax.tree.map(lambda _: vmem, out_shape),
            out_shape=out_shape,
            compiler_params=pltpu.CompilerParams(vmem_limit_bytes=16 * MIB),
            name=body.__name__,
        )(index, *operands)

    gate_pre, up_pre, split_down = kernel(
        own_half_kernel,
        [jax.ShapeDtypeStruct((slots_all, units), F32)] * 2
        + [jax.ShapeDtypeStruct((2, pairs, units, width), BF16)],
        own,
        gate,
        up,
        expert_down.reshape(units, full_width),
    )
    hidden, send = kernel(
        peer_half_kernel,
        [jax.ShapeDtypeStruct((slots_all, units), BF16), sent],
        peer,
        gate_pre,
        up_pre,
        gate,
        up,
        split_down,
    )
    arrived = swapped(send)
    keep = kernel(keep_kernel, sent, hidden, split_down)
    expert_out = (keep.astype(F32) + arrived.astype(F32)).astype(BF16)
    returned = lax.all_to_all(
        expert_out.reshape(groups * pairs, capacity, half_width // pairs),
        ("ep", "zp"),
        split_axis=0,
        concat_axis=0,
        tiled=True,
    ).reshape(pairs * slots_all, half_width // pairs)

    rows = lax.broadcasted_iota(jnp.int32, (pairs * slots_all, tok_rows), 0)
    slot_of_row = rows // (pairs * capacity) * capacity + rows % capacity
    first_back = (slot_of_row == first_place).astype(BF16)
    second_back = (slot_of_row == second_place).astype(BF16)
    contract = (((0,), (0,)), ((), ()))
    first_out = lax.dot_general(returned, first_back, contract, preferred_element_type=F32)
    second_out = lax.dot_general(returned, second_back, contract, preferred_element_type=F32)
    weights = route_weights.T
    partial = (weights[0] * first_out + weights[1] * second_out).astype(BF16)
    parts = lax.all_to_all(
        partial.reshape(columns // pairs, part_width, tok_rows),
        "z8",
        split_axis=0,
        concat_axis=0,
        tiled=True,
    )
    combined = jnp.sum(parts.astype(F32), axis=0)
    output_sq = jnp.sum(sent_to_all(jnp.sum(combined * combined, axis=0)[None], TP), axis=(0, 1))
    result = combined * lax.rsqrt(output_sq / full_width + EPSILON) * post_gain[:, None]
    return result.astype(BF16).T


def solution(mesh):
    torus = Mesh(mesh.devices.reshape(mesh.shape["ep"], 8, 2, 2), ("ep", *TP))
    in_specs = (
        P("ep", TP),
        P(TP),
        P("ep", None, TP),
        P("ep", None, TP),
        P("ep", TP, None),
        P("ep", None),
        P("ep", None),
        P(TP),
    )
    out_specs = P("ep", TP)
    return jax.shard_map(local, mesh=torus, in_specs=in_specs, out_specs=out_specs, check_vma=False)
```

time: 181 us -> 168 us (0.928)
  blocking collectives: 116 us -> 104 us
  waiting for transfers between devices: 31.6 us -> 26 us
  matrix products: 2.14 us -> 4.61 us
  local copies, waits for them, and re-layouts: 0.82 us -> 3.25 us
    all_to_all x1, blocking collectives: 29 us -> 22 us  [local(): lax.all_to_all(partial.reshape(columns // pairs, part_width, tok_rows), '...]
    all_to_all x1, blocking collectives: 25.2 us -> 20.9 us  [sent_to_all(): return lax.all_to_all(copies, axis, split_axis=0, concat_axis=0, tiled=True)]
    ppermute x3, waiting for transfers between devices: 6.58 us -> 2.8 us  [swapped(): return lax.ppermute(value, 'tp_1', [(0, 1), (1, 0)])]
    dot_general x2, matrix products: 1.36 us -> 3.82 us  [the longest x1 1.92 us: local(): lax.dot_general(returned, second_back, contract, preferred_element_type=F32)]
    unnamed x10, local copies, waits for them, and re-layouts: 0.03 us -> 2.46 us
    pallas_call x1 -> x3, Pallas kernels: 6.08 us -> 5.1 us  [kernel(): pl.pallas_call(body, in_specs=[smem] + [vmem] * len(operands), out_specs=...]
  transfers between devices with their start and end apart: 4 -> 4, of which waited for: 3 -> 2; matrix products, arithmetic and copies ran while one was open for 1% -> 1% of each run, Pallas kernels for 0% -> 1%
where the time goes in v2:
time: 168 us; the launch traced here: 167 us
  blocking collectives  104 us (62%)
  waiting for transfers between devices  26 us (15%)
  starting transfers between devices  19.5 us (12%)
  Pallas kernels  5.1 us (3%)
  matrix products  4.61 us (3%)
  other arithmetic  4.38 us (3%)
  local copies, waits for them, and re-layouts  3.25 us (2%)
    all_gather x1, blocking collectives, local(): gathered = lax.all_gather(payload, Z, axis=0, tiled=False)  32.1 us
    all_to_all x1, blocking collectives, local(): lax.all_to_all(outgoing.reshape(groups, capacity, half_width), 'ep', spli...  29.1 us
    all_to_all x1, waiting for transfers between devices, local(): lax.all_to_all(expert_out.reshape(groups * pairs, capacity, half_width //...  23.2 us
    all_to_all x1, blocking collectives, local(): lax.all_to_all(partial.reshape(columns // pairs, part_width, tok_rows), '...  22 us
    all_to_all x1, blocking collectives, sent_to_all(): return lax.all_to_all(copies, axis, split_axis=0, concat_axis=0, tiled=True)  20.9 us
    ppermute x3, starting transfers between devices, swapped(): return lax.ppermute(value, 'tp_1', [(0, 1), (1, 0)])  15.4 us
    pallas_call x3, Pallas kernels, kernel(): pl.pallas_call(body, in_specs=[smem] + [vmem] * len(operands), out_specs=...  5.1 us
    all_to_all x1, starting transfers between devices, local(): lax.all_to_all(expert_out.reshape(groups * pairs, capacity, half_width //...  4.1 us
  transfers between devices with their start and end apart: 4, of which 2 were waited for; matrix products, arithmetic and copies ran while one was open for 1% of the time, Pallas kernels for 1%

profile of v2, /device:TPU:1, one launch (start us, length us, event | category | flops | bytes accessed | tf_op | source)
XLA Modules:
  0.0 167.1 jit_solution(16868681792608094034)
XLA Ops:
  0.0 0.8 fusion.45
  0.9 32.1 %all-gather = bf16[1152,256]{1,0:T(8,128)(2,1)S(1)} all-gather(bf16[72,256]{1,0:T(8,128)(2,1)S(1)} %pad_maximum_fusion), channel_id=2, replica_groups=mesh['ep'=16,'z8'=8,'zp'=2,'tp_1'=2] {'z8','zp'}, dimensions={0}, use_global_device_ids=true | all-gather | bytes 626688 | tf_op jit(solution)/shard_map/all_gather | solution.py:109
  33.0 10.1 %collective-permute-start = (f32[1,256]{1,0:T(1,128)S(1)}, f32[1,256]{1,0:T(1,128)S(1)}, u32[]{:S(2)}, u32[]{:S(2)}) collective-permute-start(f32[1,256]{1,0:T(1,128)S(1)} %bitcast.52), channel_id=1, source_target_pairs={{0,1},{1,0},{2,3},{3,2},{4,5},{5,4},{6,7},{7,6},{8,9},{9,8},{10,11... | collective-permute-start | bytes 3080 | tf_op jit(solution)/shard_map/ppermute | solution.py:24
  43.2 0.8 fusion.65
  44.0 0.2 select_reduce_fusion.1
  44.2 0.8 multiply_add_fusion.1
  44.9 0.0 collective-permute-done
  44.9 0.1 multiply_convert_fusion
  45.1 0.6 convolution_convert_fusion
  45.7 0.0 copy-start
  45.7 29.1 %all_to_all.20 = bf16[16,48,1024]{2,1,0:T(8,128)(2,1)S(1)} all-to-all(bf16[16,48,1024]{2,1,0:T(8,128)(2,1)S(1)} %bitcast.38), channel_id=1, replica_groups=mesh['ep'=16,'z8'=8,'zp'=2,'tp_1'=2] {'ep'}, dimensions={0} | all-to-all | bytes 3145728 | tf_op jit(solution)/shard_map/all_to_all | solution.py:139
  74.8 3.3 %collective-permute-start.1 = (bf16[768,1024]{1,0:T(8,128)(2,1)S(1)}, bf16[768,1024]{1,0:T(8,128)(2,1)}, u32[]{:S(2)}, u32[]{:S(2)}) collective-permute-start(bf16[768,1024]{1,0:T(8,128)(2,1)S(1)} %bitcast.31), channel_id=1, source_target_pairs={{0,1},{1,0},{2,3},{3,2},{4,5},{5,4},{6,7},{7,6},{8,9},{9,8},{10,11... | collective-permute-start | bytes 4718600 | tf_op jit(solution)/shard_map/ppermute | solution.py:24
  78.1 0.0 copy-done
  78.1 0.0 copy-start.1
  78.1 1.2 copy-done.1
  79.3 0.0 copy-start.2
  79.4 1.2 copy-done.2
  80.6 1.6 own_half_kernel.1
  82.1 0.0 collective-permute-done.1.peer
  82.1 3.0 %peer_half_kernel.1 = (bf16[768,256]{1,0:T(8,128)(2,1)S(1)}, bf16[16,2,48,512]{3,2,1,0:T(8,128)(2,1)S(1)}) custom-call(s32[1]{0:T(128)} %bitcast.2.core, bf16[768,1024]{1,0:T(8,128)(2,1)} %collective-permute-done.1.peer, f32[768,256]{1,0:T(8,128)S(1)} %get-tuple-element.10.gate_own, f32[768,256]{1,0:T(8,128)S(1)} %get-tuple-element.11.up_own, ...), custom_call_target="tpu_custom_call" | custom-call | tf_op jit(solution)/shard_map/peer_half_kernel/pallas_call | solution.py:154
  85.1 1.9 %collective-permute-start.2 = (bf16[16,2,48,512]{3,2,1,0:T(8,128)(2,1)S(1)}, bf16[16,2,48,512]{3,2,1,0:T(8,128)(2,1)S(1)}, u32[]{:S(2)}, u32[]{:S(2)}) collective-permute-start(bf16[16,2,48,512]{3,2,1,0:T(8,128)(2,1)S(1)} %get-tuple-element.14), channel_id=1, source_target_pairs={{0,1},{1,0},{2,3},{3,2},{4,5},{5,4},{6,7},{7,6},{8,9},{9,8},{10,11... | collective-permute-start | bytes 4718600 | tf_op jit(solution)/shard_map/ppermute | solution.py:24
  87.1 0.6 keep_kernel.1
  87.6 2.8 %collective-permute-done.2 = bf16[16,2,48,512]{3,2,1,0:T(8,128)(2,1)S(1)} collective-permute-done((bf16[16,2,48,512]{3,2,1,0:T(8,128)(2,1)S(1)}, bf16[16,2,48,512]{3,2,1,0:T(8,128)(2,1)S(1)}, u32[]{:S(2)}, u32[]{:S(2)}) %collective-permute-start.2) | collective-permute-done | bytes 1572896 | tf_op jit(solution)/shard_map/ppermute | solution.py:24
  90.4 1.7 %add_convert_fusion = bf16[16,2,48,512]{3,2,1,0:T(8,128)(2,1)} fusion(bf16[16,2,48,512]{3,2,1,0:T(8,128)(2,1)S(1)} %collective-permute-done.2, bf16[16,2,48,512]{3,2,1,0:T(8,128)(2,1)S(1)} %keep_kernel.1), kind=kLoop, calls=%fused_computation | loop fusion | flops 3145728 | bytes 4718592 | tf_op jit(solution)/shard_map/convert_element_type | solution.py:184
  92.2 0.0 copy-start.3
  92.2 4.1 %all-to-all-start.1 = ((bf16[32,48,512]{2,1,0:T(8,128)(2,1)}), bf16[32,48,512]{2,1,0:T(8,128)(2,1)S(1)}, u32[]{:S(2)}, u32[]{:S(2)}) async-start(bf16[32,48,512]{2,1,0:T(8,128)(2,1)} %bitcast.21), calls=%async_computation.1 | async-start | bytes 3145728 | tf_op jit(solution)/shard_map/all_to_all | solution.py:185
  96.3 0.0 copy-done.3
  96.3 23.2 %all-to-all-done.1 = bf16[32,48,512]{2,1,0:T(8,128)(2,1)S(1)} async-done(((bf16[32,48,512]{2,1,0:T(8,128)(2,1)}), bf16[32,48,512]{2,1,0:T(8,128)(2,1)S(1)}, u32[]{:S(2)}, u32[]{:S(2)}) %all-to-all-start.1) | async-done | bytes 1572896 | tf_op jit(solution)/shard_map/all_to_all | solution.py:185
  119.5 1.9 %fusion.12 = f32[512,256]{1,0:T(8,128)S(1)} fusion(bf16[1536,512]{1,0:T(8,128)(2,1)S(1)} %bitcast.42, s32[256]{0:T(256)S(1)} %bitcast.50, s32[1536]{0:T(1024)S(1)} %get-tuple-element.28, s32[1536]{0:T(1024)S(1)} %get-tuple-element.30, s32[1536]{0:T(1024)S(1)} %get-tuple-element.29, s32[1536]{0:T(1024)S(1)} %get-tuple-element.31, ...), kind=kOutput, calls=%fused_computation.9 | convolution fusion | flops 404750336 | bytes 2126848 | tf_op jit(solution)/shard_map/dot_general | solution.py:198
  121.4 0.0 copy-start.4
  121.5 1.9 %fusion.15 = bf16[512,256]{1,0:T(8,128)(2,1)S(1)} fusion(f32[512,256]{1,0:T(8,128)S(1)} %fusion.12, bf16[1536,512]{1,0:T(8,128)(2,1)S(1)} %bitcast.43, s32[256]{0:T(256)S(1)} %bitcast.48, s32[1536]{0:T(1024)S(1)} %get-tuple-element.28, s32[1536]{0:T(1024)S(1)} %get-tuple-element.30, s32[1536]{0:T(1024)S(1)} %get-tuple-element.29, ...), kind=kOutput, calls=%fused_computation.10 | convolution fusion | flops 405012480 | bytes 2388992 | tf_op jit(solution)/shard_map/dot_general | solution.py:199
  123.4 22.0 %all_to_all.21 = bf16[8,64,256]{2,1,0:T(8,128)(2,1)S(1)} all-to-all(bf16[8,64,256]{2,1,0:T(8,128)(2,1)S(1)} %bitcast.44), channel_id=1, replica_groups=mesh['ep'=16,'z8'=8,'zp'=2,'tp_1'=2] {'z8'}, dimensions={0} | all-to-all | bytes 524288 | tf_op jit(solution)/shard_map/all_to_all | solution.py:202
  145.5 20.9 %all_to_all.22 = f32[32,1,256]{2,1,0:T(1,128)S(1)} all-to-all(f32[32,1,256]{2,1,0:T(1,128)S(1)} %broadcast_in_dim.8), channel_id=1, replica_groups=mesh['ep'=16,'z8'=8,'zp'=2,'tp_1'=2] {'z8','zp','tp_1'}, dimensions={0} | all-to-all | bytes 65536 | tf_op jit(solution)/shard_map/all_to_all | solution.py:20
  166.3 0.1 reduce_sum.72
  166.4 0.0 copy-done.4
  166.4 0.7 fusion.44
  (15 shorter events, 0.2 us)
Async XLA Ops:
  33.0 11.9 %collective-permute-start = (f32[1,256]{1,0:T(1,128)S(1)}, f32[1,256]{1,0:T(1,128)S(1)}, u32[]{:S(2)}, u32[]{:S(2)}) collective-permute-start(f32[1,256]{1,0:T(1,128)S(1)} %bitcast.52), channel_id=1, source_target_pairs={{0,1},{1,0},{2,3},{3,2},{4,5},{5,4},{6,7},{7,6},{8,9},{9,8},{10,11... | collective-permute-start | bytes 3080 | tf_op jit(solution)/shard_map/ppermute | solution.py:24
  45.7 32.4 %copy-start = (bf16[1,2048,256]{2,1,0:T(8,128)(2,1)S(1)}, bf16[1,2048,256]{2,1,0:T(8,128)(2,1)}, u32[]{:S(2)}) copy-start(bf16[1,2048,256]{2,1,0:T(8,128)(2,1)} %param.10) | copy-start | bytes 3145732
  74.8 7.4 %collective-permute-start.1 = (bf16[768,1024]{1,0:T(8,128)(2,1)S(1)}, bf16[768,1024]{1,0:T(8,128)(2,1)}, u32[]{:S(2)}, u32[]{:S(2)}) collective-permute-start(bf16[768,1024]{1,0:T(8,128)(2,1)S(1)} %bitcast.31), channel_id=1, source_target_pairs={{0,1},{1,0},{2,3},{3,2},{4,5},{5,4},{6,7},{7,6},{8,9},{9,8},{10,11... | collective-permute-start | bytes 4718600 | tf_op jit(solution)/shard_map/ppermute | solution.py:24
  78.1 1.2 copy-start.1
  79.3 1.2 copy-start.2
  85.1 5.3 %collective-permute-start.2 = (bf16[16,2,48,512]{3,2,1,0:T(8,128)(2,1)S(1)}, bf16[16,2,48,512]{3,2,1,0:T(8,128)(2,1)S(1)}, u32[]{:S(2)}, u32[]{:S(2)}) collective-permute-start(bf16[16,2,48,512]{3,2,1,0:T(8,128)(2,1)S(1)} %get-tuple-element.14), channel_id=1, source_target_pairs={{0,1},{1,0},{2,3},{3,2},{4,5},{5,4},{6,7},{7,6},{8,9},{9,8},{10,11... | collective-permute-start | bytes 4718600 | tf_op jit(solution)/shard_map/ppermute | solution.py:24
  92.2 4.2 %copy-start.3 = (f32[256,2]{0,1:T(2,128)S(1)}, f32[256,2]{0,1:T(2,128)}, u32[]{:S(2)}) copy-start(f32[256,2]{0,1:T(2,128)} %param.14) | copy-start | bytes 6148
  92.2 27.4 %all-to-all-start.1 = ((bf16[32,48,512]{2,1,0:T(8,128)(2,1)}), bf16[32,48,512]{2,1,0:T(8,128)(2,1)S(1)}, u32[]{:S(2)}, u32[]{:S(2)}) async-start(bf16[32,48,512]{2,1,0:T(8,128)(2,1)} %bitcast.21), calls=%async_computation.1 | async-start | bytes 3145728 | tf_op jit(solution)/shard_map/all_to_all | solution.py:185
  121.4 45.0 %copy-start.4 = (f32[64]{0:T(128)S(1)}, f32[64]{0:T(128)}, u32[]{:S(2)}) copy-start(f32[64]{0:T(128)} %param.15) | copy-start | bytes 772

commit v3 on v1

v3 whole, which is shorter than its diff:
```python
import jax
import jax.numpy as jnp
from jax import lax
from jax.experimental import pallas as pl
from jax.experimental.pallas import tpu as pltpu
from jax.sharding import Mesh
from jax.sharding import PartitionSpec as P

Z = ("z8", "zp")
TP = ("z8", "zp", "core")
EPSILON = 1e-06
F32 = jnp.float32
BF16 = jnp.bfloat16
MIB = 1024 * 1024
VMEM = pl.BlockSpec(memory_space=pltpu.VMEM)
HBM = pl.BlockSpec(memory_space=pltpu.HBM)


def exchanged(value, axis):
    return lax.all_to_all(value, axis, split_axis=0, concat_axis=0, tiled=True)


def swapped(value):
    return lax.ppermute(value, "core", [(0, 1), (1, 0)])


def three_pieces(value):
    high = lax.reduce_precision(value, 8, 7)
    middle = lax.reduce_precision(value - high, 8, 7)
    low = lax.reduce_precision(value - high - middle, 8, 7)
    return jnp.stack([high, middle, low]).astype(BF16)


def in_hbm(value):
    return pltpu.with_memory_space_constraint(value, pltpu.HBM)


def kernel(body, out_shape, *operands, in_specs=None, out_specs=VMEM, scratch_shapes=()):
    return pl.pallas_call(
        body,
        in_specs=in_specs or [VMEM] * len(operands),
        out_specs=out_specs,
        out_shape=out_shape,
        scratch_shapes=scratch_shapes,
        compiler_params=pltpu.CompilerParams(vmem_limit_bytes=16 * MIB),
    )(*operands)


def slots_kernel(chosen, places):
    tok_rows = chosen.shape[1]
    groups = 16
    few = 3 * tok_rows // groups // 2
    experts = lax.broadcasted_iota(jnp.int32, (groups, tok_rows), 0)
    hot = [(experts == chosen[k : k + 1, :]).astype(F32) for k in range(2)]
    before = (
        lax.broadcasted_iota(jnp.int32, (tok_rows, tok_rows), 0)
        < lax.broadcasted_iota(jnp.int32, (tok_rows, tok_rows), 1)
    ).astype(F32)
    earlier = jnp.dot(
        (hot[0] + hot[1]).astype(BF16), before.astype(BF16), preferred_element_type=F32
    )
    for k in range(2):
        slot = jnp.sum(earlier * hot[k], axis=0, keepdims=True).astype(jnp.int32)
        upper = (slot >= few).astype(jnp.int32)
        places[k : k + 1, :] = (
            upper * (groups * few) + chosen[k : k + 1, :] * few + slot - upper * few
        )


def reorder_kernel(down, split_down, held, turned, sems):
    coming = pltpu.make_async_copy(down, held, sems.at[0])
    coming.start()
    size = 512
    row = lax.broadcasted_iota(jnp.int32, (size, size), 0)
    col = lax.broadcasted_iota(jnp.int32, (size, size), 1)
    part = col // 64
    source = (part % 2) * 256 + (part // 2) * 64 + col % 64
    shuffle = (row == source).astype(F32).astype(BF16)
    coming.wait()
    for block in range(held.shape[1] // size):
        value = jnp.dot(
            held[:, block * size : (block + 1) * size], shuffle, preferred_element_type=F32
        ).astype(BF16)
        for part in range(4):
            turned[part, :, block * 128 : block * 128 + 128] = value[
                :, part * 128 : part * 128 + 128
            ]
    leaving = pltpu.make_async_copy(turned, split_down, sems.at[1])
    leaving.start()
    leaving.wait()


def expert_kernel(
    rows, gate_own, up_own, gate_peer, up_peer, down_own, down_peer, sent, *scratch
):
    held, sems = scratch[:-1], scratch[-1]
    copies = [
        pltpu.make_async_copy(source, target, sems.at[k])
        for k, (source, target) in enumerate(
            zip((gate_own, up_own, gate_peer, up_peer, down_own, down_peer), held)
        )
    ]
    for copy in copies:
        copy.start()
    half, units = rows.shape[2], gate_own.shape[-1]
    step = 192
    starts = range(0, rows.shape[1], step)
    hidden = {}
    for which in range(2):
        gate, up = held[2 * which], held[2 * which + 1]
        copies[2 * which].wait()
        copies[2 * which + 1].wait()
        for start in starts:
            here = slice(start, start + step)
            gate_pre = up_pre = None
            for side in range(2):
                value = rows[side, here, :]
                more_gate = jnp.dot(
                    value, gate[:, side].reshape(half, units), preferred_element_type=F32
                )
                more_up = jnp.dot(
                    value, up[:, side].reshape(half, units), preferred_element_type=F32
                )
                gate_pre = more_gate if gate_pre is None else gate_pre + more_gate
                up_pre = more_up if up_pre is None else up_pre + more_up
            hidden[which, start] = (gate_pre / (1.0 + jnp.exp(-gate_pre)) * up_pre).astype(BF16)
    copies[4].wait()
    copies[5].wait()
    for start in starts:
        here = slice(start, start + step)
        for part in range(4):
            out = jnp.dot(hidden[0, start], held[4][part], preferred_element_type=F32)
            out = out + jnp.dot(hidden[1, start], held[5][part], preferred_element_type=F32)
            sent[part, here, :] = out.astype(BF16)


def combine_kernel(returned, places, weights, partial):
    slots_all, tok_rows = returned.shape[1], places.shape[1]
    slots = lax.broadcasted_iota(jnp.int32, (slots_all, tok_rows), 0)
    both = (returned[0].astype(F32) + returned[1].astype(F32)).astype(BF16)
    total = None
    for k in range(2):
        hot = (slots == places[k : k + 1, :]).astype(F32).astype(BF16)
        picked = lax.dot_general(
            both, hot, (((0,), (0,)), ((), ())), preferred_element_type=F32
        )
        picked = picked * weights[k : k + 1, :]
        total = picked if total is None else total + picked
    partial[...] = total.astype(BF16)


def local(tokens, pre_gain, expert_gate, expert_up, expert_down, routes, route_weights, post_gain):
    groups = lax.axis_size("ep")
    columns = lax.axis_size(Z)
    tok_rows, part_width = tokens.shape
    full_width = part_width * lax.axis_size(TP)
    half_width = full_width // 2
    width = full_width // 4
    few = 3 * tok_rows // groups // 2
    slots_all = 2 * groups * few
    units = expert_gate.shape[-1]

    values = tokens.T.astype(F32)
    partial_sq = jnp.sum(values * values, axis=0)
    scaled = (values * pre_gain[:, None]).astype(BF16)
    pieces = jnp.pad(three_pieces(partial_sq), ((0, 5), (0, 0)))
    payload = jnp.concatenate([scaled, pieces], axis=0)
    gathered = lax.all_gather(payload, Z, axis=0, tiled=False)
    half_sq = jnp.sum(gathered[:, part_width : part_width + 3].astype(F32), axis=(0, 1))
    input_sq = half_sq + swapped(half_sq[None])[0]
    row_scale = lax.rsqrt(input_sq / full_width + EPSILON)
    normed = (
        (gathered[:, :part_width].astype(F32) * row_scale).astype(BF16).reshape(half_width, tok_rows)
    )

    places = kernel(slots_kernel, jax.ShapeDtypeStruct((2, tok_rows), jnp.int32), routes.T)
    slots = lax.broadcasted_iota(jnp.int32, (slots_all, tok_rows), 0)
    dispatch = (slots == places[0]).astype(BF16) + (slots == places[1]).astype(BF16)
    outgoing = lax.dot_general(
        dispatch, normed, (((1,), (1,)), ((), ())), preferred_element_type=F32
    ).astype(BF16)
    rows = exchanged(outgoing.reshape(2 * groups, few, half_width), ("core", "ep"))

    gate = expert_gate.reshape(columns, 2, part_width, units)
    up = expert_up.reshape(columns, 2, part_width, units)
    down = kernel(
        reorder_kernel,
        pltpu.HBM((4, units, width), BF16),
        in_hbm(expert_down.reshape(units, full_width)),
        in_specs=[HBM],
        out_specs=HBM,
        scratch_shapes=[
            pltpu.VMEM((units, full_width), BF16),
            pltpu.VMEM((4, units, width), BF16),
            pltpu.SemaphoreType.DMA((2,)),
        ],
    )
    gate_peer = swapped(gate)
    up_peer = swapped(up)
    down_peer = swapped(down)
    sent = kernel(
        expert_kernel,
        jax.ShapeDtypeStruct((4, groups * few, width), BF16),
        rows.reshape(2, groups * few, half_width),
        *(in_hbm(w) for w in (gate, up, gate_peer, up_peer, down, down_peer)),
        in_specs=[VMEM] + [HBM] * 6,
        scratch_shapes=[pltpu.VMEM(gate.shape, BF16)] * 4
        + [pltpu.VMEM(down.shape, BF16)] * 2
        + [pltpu.SemaphoreType.DMA((6,))],
    )
    returned = exchanged(sent.reshape(4 * groups, few, width), ("zp", "core", "ep"))

    partial = kernel(
        combine_kernel,
        jax.ShapeDtypeStruct((width, tok_rows), BF16),
        returned.reshape(2, slots_all, width),
        places,
        route_weights.T,
    )
    parts = exchanged(partial.reshape(columns // 2, part_width, tok_rows), "z8")
    combined = jnp.sum(parts.astype(F32), axis=0)
    own_sq = jnp.sum(combined * combined, axis=0)
    copies = jnp.broadcast_to(own_sq[None, None], (lax.axis_size(TP), 1, tok_rows))
    output_sq = jnp.sum(exchanged(copies, TP), axis=(0, 1))
    result = combined * lax.rsqrt(output_sq / full_width + EPSILON) * post_gain[:, None]
    return result.astype(BF16).T


def solution(mesh):
    torus = Mesh(mesh.devices.reshape(mesh.shape["ep"], 8, 2, 2), ("ep", *TP))
    in_specs = (
        P("ep", TP),
        P(TP),
        P("ep", None, TP),
        P("ep", None, TP),
        P("ep", TP, None),
        P("ep", None),
        P("ep", None),
        P(TP),
    )

    return jax.shard_map(
        local, mesh=torus, in_specs=in_specs, out_specs=P("ep", TP), check_vma=False
    )
```

time: 181 us -> 154 us (0.85)
  waiting for transfers between devices: 31.6 us -> 11 us
  blocking collectives: 116 us -> 103 us
  starting transfers between devices: 19.6 us -> 24 us
  other arithmetic: 4.51 us -> 1.85 us
  Pallas kernels: 6.08 us -> 8.52 us
    all_to_all x1, waiting for transfers between devices: 25 us -> 10.3 us  [exchanged(): return lax.all_to_all(value, axis, split_axis=0, concat_axis=0, tiled=True)]
    all_to_all x3, blocking collectives: 83.5 us -> 71.2 us  [exchanged(): return lax.all_to_all(value, axis, split_axis=0, concat_axis=0, tiled=True)]
    ppermute x3 -> x4, waiting for transfers between devices: 6.58 us -> 0.72 us  [swapped(): return lax.ppermute(value, 'core', [(0, 1), (1, 0)])]
    all_to_all x1, starting transfers between devices: 3.84 us -> 7.35 us  [exchanged(): return lax.all_to_all(value, axis, split_axis=0, concat_axis=0, tiled=True)]
    unnamed x10 -> x14, local copies, waits for them, and re-layouts: 0.03 us -> 2.51 us
    pallas_call x1 -> x4, Pallas kernels: 6.08 us -> 8.52 us  [kernel(): pl.pallas_call(body, in_specs=in_specs or [VMEM] * len(operands), out_spe...]
    convert_element_type x3 -> x0, other arithmetic: 1.86 us -> none  [the longest x1 1.85 us: local(): expert_out = (keep.astype(F32) + swapped(send).astype(F32)).astype(BF16)]
    ppermute x3 -> x4, starting transfers between devices: 15.8 us -> 16.6 us  [swapped(): return lax.ppermute(value, 'core', [(0, 1), (1, 0)])]
  transfers between devices with their start and end apart: 4 -> 5, of which waited for: 3 -> 3; matrix products, arithmetic and copies ran while one was open for 1% -> 0% of each run, Pallas kernels for 0% -> 2%
where the time goes in v3:
time: 154 us; the launch traced here: 153 us
  blocking collectives  103 us (67%)
  starting transfers between devices  24 us (16%)
  waiting for transfers between devices  11 us (7%)
  Pallas kernels  8.52 us (6%)
  local copies, waits for them, and re-layouts  2.53 us (2%)
  other arithmetic  1.85 us (1%)
  matrix products  1.78 us (1%)
    all_to_all x3, blocking collectives, exchanged(): return lax.all_to_all(value, axis, split_axis=0, concat_axis=0, tiled=True)  71.2 us
    all_gather x1, blocking collectives, local(): gathered = lax.all_gather(payload, Z, axis=0, tiled=False)  32.1 us
    ppermute x4, starting transfers between devices, swapped(): return lax.ppermute(value, 'core', [(0, 1), (1, 0)])  16.6 us
    all_to_all x1, waiting for transfers between devices, exchanged(): return lax.all_to_all(value, axis, split_axis=0, concat_axis=0, tiled=True)  10.3 us
    pallas_call x4, Pallas kernels, kernel(): pl.pallas_call(body, in_specs=in_specs or [VMEM] * len(operands), out_spe...  8.52 us
    all_to_all x1, starting transfers between devices, exchanged(): return lax.all_to_all(value, axis, split_axis=0, concat_axis=0, tiled=True)  7.35 us
  transfers between devices with their start and end apart: 5, of which 3 were waited for; matrix products, arithmetic and copies ran while one was open for 0% of the time, Pallas kernels for 2%

profile of v3, /device:TPU:1, one launch (start us, length us, event | category | flops | bytes accessed | tf_op | source)
XLA Modules:
  0.0 153.2 jit_solution(11938982369241526569)
XLA Ops:
  0.0 0.8 fusion.10
  0.9 32.1 %all-gather = bf16[1152,256]{1,0:T(8,128)(2,1)S(1)} all-gather(bf16[72,256]{1,0:T(8,128)(2,1)S(1)} %pad_maximum_fusion), channel_id=2, replica_groups=mesh['ep'=16,'z8'=8,'zp'=2,'core'=2] {'z8','zp'}, dimensions={0}, use_global_device_ids=true | all-gather | bytes 626688 | tf_op jit(solution)/shard_map/all_gather | solution.py:168
  33.0 10.1 %collective-permute-start = (f32[1,256]{1,0:T(1,128)S(1)}, f32[1,256]{1,0:T(1,128)S(1)}, u32[]{:S(2)}, u32[]{:S(2)}) collective-permute-start(f32[1,256]{1,0:T(1,128)S(1)} %bitcast.39), channel_id=1, source_target_pairs={{0,1},{1,0},{2,3},{3,2},{4,5},{5,4},{6,7},{7,6},{8,9},{9,8},{10,11... | collective-permute-start | bytes 3080 | tf_op jit(solution)/shard_map/ppermute | solution.py:24
  43.2 0.0 copy-start.1
  43.2 0.7 copy-done.1
  43.9 0.2 shard_map.82.places
  44.1 0.0 collective-permute-done
  44.1 0.1 multiply_convert_fusion
  44.2 1.8 %convolution_convert_fusion = bf16[768,1024]{1,0:T(8,128)(2,1)} fusion(bf16[1024,256]{1,0:T(8,128)(2,1)S(1)} %bitcast.30, s32[256]{0:T(256)S(1)} %bitcast.37, s32[256]{0:T(256)S(1)} %bitcast.36), kind=kOutput, calls=%fused_computation | convolution fusion | flops 405012480 | bytes 2099200 | tf_op jit(solution)/shard_map/dot_general | solution.py:179
  46.0 7.3 %all-to-all-start = ((bf16[32,24,1024]{2,1,0:T(8,128)(2,1)}), bf16[32,24,1024]{2,1,0:T(8,128)(2,1)S(1)}, u32[]{:S(2)}, u32[]{:S(2)}) async-start(bf16[32,24,1024]{2,1,0:T(8,128)(2,1)} %bitcast.9), calls=%async_computation | async-start | bytes 3145728 | tf_op jit(solution)/shard_map/all_to_all | solution.py:20
  53.4 0.0 copy-start.2
  53.4 0.0 copy-start.3
  53.4 3.1 %shard_map.83.down_own = bf16[4,256,512]{2,1,0:T(8,128)(2,1)} custom-call(bf16[256,2048]{1,0:T(8,128)(2,1)} %bitcast.35), custom_call_target="tpu_custom_call" | custom-call | tf_op jit(solution)/shard_map/pallas_call | solution.py:39
  56.4 2.1 %collective-permute-start.3 = (bf16[4,256,512]{2,1,0:T(8,128)(2,1)}, bf16[4,256,512]{2,1,0:T(8,128)(2,1)S(1)}, u32[]{:S(2)}, u32[]{:S(2)}) collective-permute-start(bf16[4,256,512]{2,1,0:T(8,128)(2,1)} %shard_map.83.down_own), channel_id=1, source_target_pairs={{0,1},{1,0},{2,3},{3,2},{4,5},{5,4},{6,7},{7,6},{8,9},{9,8},{10,11... | collective-permute-start | bytes 3145736 | tf_op jit(solution)/shard_map/ppermute | solution.py:24
  58.6 0.0 copy-done.2
  58.6 2.2 %collective-permute-start.1 = (bf16[16,2,64,256]{3,2,1,0:T(8,128)(2,1)S(1)}, bf16[16,2,64,256]{3,2,1,0:T(8,128)(2,1)S(1)}, u32[]{:S(2)}, u32[]{:S(2)}) collective-permute-start(bf16[16,2,64,256]{3,2,1,0:T(8,128)(2,1)S(1)} %bitcast.32), channel_id=1, source_target_pairs={{0,1},{1,0},{2,3},{3,2},{4,5},{5,4},{6,7},{7,6},{8,9},{9,8},{10,11... | collective-permute-start | bytes 3145736 | tf_op jit(solution)/shard_map/ppermute | solution.py:24
  60.8 0.0 copy-done.3
  60.8 2.1 %collective-permute-start.2 = (bf16[16,2,64,256]{3,2,1,0:T(8,128)(2,1)S(1)}, bf16[16,2,64,256]{3,2,1,0:T(8,128)(2,1)}, u32[]{:S(2)}, u32[]{:S(2)}) collective-permute-start(bf16[16,2,64,256]{3,2,1,0:T(8,128)(2,1)S(1)} %bitcast.34), channel_id=1, source_target_pairs={{0,1},{1,0},{2,3},{3,2},{4,5},{5,4},{6,7},{7,6},{8,9},{9,8},{10,11... | collective-permute-start | bytes 3145736 | tf_op jit(solution)/shard_map/ppermute | solution.py:24
  62.9 0.0 collective-permute-done.3.down_peer
  63.0 0.0 copy-start.4
  63.0 0.2 collective-permute-done.1.gate_peer
  63.2 0.8 copy-done.4
  64.0 0.0 copy-start.5
  64.0 1.0 copy-done.5
  65.0 0.5 collective-permute-done.2.up_peer
  65.5 10.3 %all-to-all-done = bf16[32,24,1024]{2,1,0:T(8,128)(2,1)S(1)} async-done(((bf16[32,24,1024]{2,1,0:T(8,128)(2,1)}), bf16[32,24,1024]{2,1,0:T(8,128)(2,1)S(1)}, u32[]{:S(2)}, u32[]{:S(2)}) %all-to-all-start) | async-done | bytes 1572896 | tf_op jit(solution)/shard_map/all_to_all | solution.py:20
  75.8 4.7 %shard_map.84 = bf16[4,384,512]{2,1,0:T(8,128)(2,1)S(1)} custom-call(bf16[2,384,1024]{2,1,0:T(8,128)(2,1)S(1)} %bitcast.22, bf16[16,2,64,256]{3,2,1,0:T(8,128)(2,1)} %bitcast.31, bf16[16,2,64,256]{3,2,1,0:T(8,128)(2,1)} %bitcast.33, bf16[16,2,64,256]{3,2,1,0:T(8,128)(2,1)} %copy-done.5, bf16[16,2,64,256]{3,2,1,0:T(8,128)(2,1)} %collective-permute-done.2.up_peer, ...), custom_call_target="tpu_custom_call" | custom-call | tf_op jit(solution)/shard_map/pallas_call | solution.py:39
  80.5 0.0 copy-start
  80.5 27.5 %all_to_all.20 = bf16[64,24,512]{2,1,0:T(8,128)(2,1)S(1)} all-to-all(bf16[64,24,512]{2,1,0:T(8,128)(2,1)S(1)} %bitcast.23), channel_id=1, replica_groups=mesh['ep'=16,'z8'=8,'zp'=2,'core'=2] {'zp','core','ep'}, dimensions={0} | all-to-all | bytes 3145728 | tf_op jit(solution)/shard_map/all_to_all | solution.py:20
  107.9 0.0 copy-start.6
  107.9 0.0 copy-done
  107.9 0.6 shard_map.85
  108.6 24.2 %all_to_all.21 = bf16[8,64,256]{2,1,0:T(8,128)(2,1)S(1)} all-to-all(bf16[8,64,256]{2,1,0:T(8,128)(2,1)S(1)} %bitcast.25), channel_id=1, replica_groups=mesh['ep'=16,'z8'=8,'zp'=2,'core'=2] {'z8'}, dimensions={0} | all-to-all | bytes 524288 | tf_op jit(solution)/shard_map/all_to_all | solution.py:20
  132.9 19.5 %all_to_all.22 = f32[32,1,256]{2,1,0:T(1,128)S(1)} all-to-all(f32[32,1,256]{2,1,0:T(1,128)S(1)} %broadcast_in_dim.5), channel_id=1, replica_groups=mesh['ep'=16,'z8'=8,'zp'=2,'core'=2] {'z8','zp','core'}, dimensions={0} | all-to-all | bytes 65536 | tf_op jit(solution)/shard_map/all_to_all | solution.py:20
  152.4 0.1 reduce_sum.52
  152.4 0.0 copy-done.6
  152.5 0.7 fusion.9
  (10 shorter events, 0.2 us)
Async XLA Ops:
  33.0 11.0 %collective-permute-start = (f32[1,256]{1,0:T(1,128)S(1)}, f32[1,256]{1,0:T(1,128)S(1)}, u32[]{:S(2)}, u32[]{:S(2)}) collective-permute-start(f32[1,256]{1,0:T(1,128)S(1)} %bitcast.39), channel_id=1, source_target_pairs={{0,1},{1,0},{2,3},{3,2},{4,5},{5,4},{6,7},{7,6},{8,9},{9,8},{10,11... | collective-permute-start | bytes 3080 | tf_op jit(solution)/shard_map/ppermute | solution.py:24
  43.2 0.7 copy-start.1
  46.0 29.8 %all-to-all-start = ((bf16[32,24,1024]{2,1,0:T(8,128)(2,1)}), bf16[32,24,1024]{2,1,0:T(8,128)(2,1)S(1)}, u32[]{:S(2)}, u32[]{:S(2)}) async-start(bf16[32,24,1024]{2,1,0:T(8,128)(2,1)} %bitcast.9), calls=%async_computation | async-start | bytes 3145728 | tf_op jit(solution)/shard_map/all_to_all | solution.py:20
  53.4 5.2 %copy-start.2 = (bf16[1,2048,256]{2,1,0:T(8,128)(2,1)S(1)}, bf16[1,2048,256]{2,1,0:T(8,128)(2,1)}, u32[]{:S(2)}) copy-start(bf16[1,2048,256]{2,1,0:T(8,128)(2,1)} %param.10) | copy-start | bytes 3145732
  53.4 7.4 %copy-start.3 = (bf16[1,2048,256]{2,1,0:T(8,128)(2,1)S(1)}, bf16[1,2048,256]{2,1,0:T(8,128)(2,1)}, u32[]{:S(2)}) copy-start(bf16[1,2048,256]{2,1,0:T(8,128)(2,1)} %param.11) | copy-start | bytes 3145732
  56.4 6.5 %collective-permute-start.3 = (bf16[4,256,512]{2,1,0:T(8,128)(2,1)}, bf16[4,256,512]{2,1,0:T(8,128)(2,1)S(1)}, u32[]{:S(2)}, u32[]{:S(2)}) collective-permute-start(bf16[4,256,512]{2,1,0:T(8,128)(2,1)} %shard_map.83.down_own), channel_id=1, source_target_pairs={{0,1},{1,0},{2,3},{3,2},{4,5},{5,4},{6,7},{7,6},{8,9},{9,8},{10,11... | collective-permute-start | bytes 3145736 | tf_op jit(solution)/shard_map/ppermute | solution.py:24
  58.6 4.6 %collective-permute-start.1 = (bf16[16,2,64,256]{3,2,1,0:T(8,128)(2,1)S(1)}, bf16[16,2,64,256]{3,2,1,0:T(8,128)(2,1)S(1)}, u32[]{:S(2)}, u32[]{:S(2)}) collective-permute-start(bf16[16,2,64,256]{3,2,1,0:T(8,128)(2,1)S(1)} %bitcast.32), channel_id=1, source_target_pairs={{0,1},{1,0},{2,3},{3,2},{4,5},{5,4},{6,7},{7,6},{8,9},{9,8},{10,11... | collective-permute-start | bytes 3145736 | tf_op jit(solution)/shard_map/ppermute | solution.py:24
  60.8 4.7 %collective-permute-start.2 = (bf16[16,2,64,256]{3,2,1,0:T(8,128)(2,1)S(1)}, bf16[16,2,64,256]{3,2,1,0:T(8,128)(2,1)}, u32[]{:S(2)}, u32[]{:S(2)}) collective-permute-start(bf16[16,2,64,256]{3,2,1,0:T(8,128)(2,1)S(1)} %bitcast.34), channel_id=1, source_target_pairs={{0,1},{1,0},{2,3},{3,2},{4,5},{5,4},{6,7},{7,6},{8,9},{9,8},{10,11... | collective-permute-start | bytes 3145736 | tf_op jit(solution)/shard_map/ppermute | solution.py:24
  63.0 1.0 copy-start.4
  64.0 1.0 copy-start.5
  80.5 27.5 %copy-start = (f32[256,2]{0,1:T(2,128)S(1)}, f32[256,2]{0,1:T(2,128)}, u32[]{:S(2)}) copy-start(f32[256,2]{0,1:T(2,128)} %param.14) | copy-start | bytes 6148
  107.9 44.5 %copy-start.6 = (f32[64]{0:T(128)S(1)}, f32[64]{0:T(128)}, u32[]{:S(2)}) copy-start(f32[64]{0:T(128)} %param.15) | copy-start | bytes 772

commit v4 on v3

v4 whole, which is shorter than its diff:
```python
import jax
import jax.numpy as jnp
from jax import lax
from jax.experimental import pallas as pl
from jax.experimental.pallas import tpu as pltpu
from jax.sharding import Mesh
from jax.sharding import PartitionSpec as P

TP = ("z8", "zp", "core")
EPSILON = 1e-06
F32 = jnp.float32
BF16 = jnp.bfloat16
MIB = 1024 * 1024
VMEM = pl.BlockSpec(memory_space=pltpu.VMEM)
HBM = pl.BlockSpec(memory_space=pltpu.HBM)


def exchanged(value, axis):
    return lax.all_to_all(value, axis, split_axis=0, concat_axis=0, tiled=True)


def swapped(value):
    return lax.ppermute(value, "core", [(0, 1), (1, 0)])


def three_pieces(value):
    high = lax.reduce_precision(value, 8, 7)
    middle = lax.reduce_precision(value - high, 8, 7)
    low = lax.reduce_precision(value - high - middle, 8, 7)
    return jnp.stack([high, middle, low]).astype(BF16)


def in_hbm(value):
    return pltpu.with_memory_space_constraint(value, pltpu.HBM)


def kernel(body, out_shape, *operands, in_specs=None, out_specs=None, scratch_shapes=()):
    return pl.pallas_call(
        body,
        in_specs=in_specs or [VMEM] * len(operands),
        out_specs=out_specs or jax.tree.map(lambda _: VMEM, out_shape),
        out_shape=out_shape,
        scratch_shapes=scratch_shapes,
        compiler_params=pltpu.CompilerParams(vmem_limit_bytes=16 * MIB),
    )(*operands)


def slots_kernel(chosen, places, dispatch):
    slots_all, tok_rows = dispatch.shape
    groups = 16
    few = slots_all // groups // 2
    experts = lax.broadcasted_iota(jnp.int32, (groups, tok_rows), 0)
    hot = [(experts == chosen[k : k + 1, :]).astype(F32) for k in range(2)]
    before = (
        lax.broadcasted_iota(jnp.int32, (tok_rows, tok_rows), 0)
        < lax.broadcasted_iota(jnp.int32, (tok_rows, tok_rows), 1)
    ).astype(F32)
    earlier = jnp.dot(
        (hot[0] + hot[1]).astype(BF16), before.astype(BF16), preferred_element_type=F32
    )
    slots = lax.broadcasted_iota(jnp.int32, (slots_all, tok_rows), 0)
    taken = None
    for k in range(2):
        slot = jnp.sum(earlier * hot[k], axis=0, keepdims=True).astype(jnp.int32)
        upper = (slot >= few).astype(jnp.int32)
        place = upper * (groups * few) + chosen[k : k + 1, :] * few + slot - upper * few
        places[k : k + 1, :] = place
        here = slots == place
        taken = here if taken is None else taken | here
    dispatch[...] = taken.astype(F32).astype(BF16)


def dispatch_kernel(dispatch, gathered, outgoing):
    part_width = 64
    columns, _, tok_rows = gathered.shape
    features = gathered[:, :part_width, :].reshape(columns * part_width, tok_rows)
    value = lax.dot_general(
        dispatch[...], features, (((1,), (1,)), ((), ())), preferred_element_type=F32
    ).astype(BF16)
    outgoing[0] = value
    outgoing[1] = value


def reorder_kernel(down, split_down, held, turned, sems):
    coming = pltpu.make_async_copy(down, held, sems.at[0])
    coming.start()
    size = 512
    row = lax.broadcasted_iota(jnp.int32, (size, size), 0)
    col = lax.broadcasted_iota(jnp.int32, (size, size), 1)
    part = col // 64
    source = (part % 2) * 256 + (part // 2) * 64 + col % 64
    shuffle = (row == source).astype(F32).astype(BF16)
    coming.wait()
    for block in range(held.shape[1] // size):
        value = jnp.dot(
            held[:, block * size : (block + 1) * size], shuffle, preferred_element_type=F32
        ).astype(BF16)
        for part in range(4):
            turned[part, :, block * 128 : block * 128 + 128] = value[
                :, part * 128 : part * 128 + 128
            ]
    leaving = pltpu.make_async_copy(turned, split_down, sems.at[1])
    leaving.start()
    leaving.wait()


def expert_kernel(
    rows, gain, gate_own, up_own, gate_peer, up_peer, down_own, down_peer, sent, *scratch
):
    gates, ups, downs, scaled, sems = scratch
    parts, length, width = rows.shape
    units = gate_own.shape[-1]
    copies = [[], [], []]
    for stage, pairs in enumerate(((gate_own, up_own), (gate_peer, up_peer))):
        for k, (source, target) in enumerate(zip(pairs, (gates, ups))):
            for part in range(parts):
                copies[stage].append(
                    pltpu.make_async_copy(
                        source.at[:, part], target.at[stage, part], sems.at[stage, k, part]
                    )
                )
    for k, source in enumerate((down_own, down_peer)):
        copies[2].append(pltpu.make_async_copy(source, downs.at[k], sems.at[2, k, 0]))
    for stage in copies:
        for copy in stage:
            copy.start()
    step = 192
    starts = range(0, length, step)
    row_scale = {}
    for start in starts:
        here = slice(start, start + step)
        square = None
        for part in range(parts):
            value = rows[part, here, :].astype(F32)
            more = value * value
            square = more if square is None else square + more
            scaled[here, part * width : (part + 1) * width] = (
                value * gain[part : part + 1, :]
            ).astype(BF16)
        mean = jnp.sum(square, axis=1, keepdims=True) / (parts * width)
        row_scale[start] = lax.rsqrt(mean + EPSILON)
    hidden = {}
    for which in range(2):
        for copy in copies[which]:
            copy.wait()
        gate = gates[which].reshape(parts * width, units)
        up = ups[which].reshape(parts * width, units)
        for start in starts:
            value = scaled[start : start + step, :]
            gate_pre = jnp.dot(value, gate, preferred_element_type=F32) * row_scale[start]
            up_pre = jnp.dot(value, up, preferred_element_type=F32) * row_scale[start]
            hidden[which, start] = (gate_pre / (1.0 + jnp.exp(-gate_pre)) * up_pre).astype(BF16)
    for copy in copies[2]:
        copy.wait()
    for start in starts:
        here = slice(start, start + step)
        for part in range(parts):
            out = jnp.dot(hidden[0, start], downs[0, part], preferred_element_type=F32)
            out = out + jnp.dot(hidden[1, start], downs[1, part], preferred_element_type=F32)
            sent[part, here, :] = out.astype(BF16)


def combine_kernel(returned, places, weights, partial):
    slots_all, tok_rows = returned.shape[1], places.shape[1]
    slots = lax.broadcasted_iota(jnp.int32, (slots_all, tok_rows), 0)
    both = (returned[0].astype(F32) + returned[1].astype(F32)).astype(BF16)
    total = None
    for k in range(2):
        hot = (slots == places[k : k + 1, :]).astype(F32).astype(BF16)
        picked = lax.dot_general(
            both, hot, (((0,), (0,)), ((), ())), preferred_element_type=F32
        )
        picked = picked * weights[k : k + 1, :]
        total = picked if total is None else total + picked
    partial[...] = total.astype(BF16)


def local(tokens, pre_gain, expert_gate, expert_up, expert_down, routes, route_weights, post_gain):
    groups = lax.axis_size("ep")
    columns = lax.axis_size("z8")
    tok_rows, part_width = tokens.shape
    full_width = part_width * lax.axis_size(TP)
    width = full_width // 4
    few = 3 * tok_rows // groups // 2
    slots_all = 2 * groups * few
    units = expert_gate.shape[-1]

    pieces = jnp.pad(three_pieces(pre_gain).reshape(1, -1), ((0, 7), (0, tok_rows - 3 * part_width)))
    payload = jnp.concatenate([tokens.T, pieces], axis=0)
    copies = jnp.broadcast_to(payload, (columns, *payload.shape))
    gathered = exchanged(copies, "z8")

    places, dispatch = kernel(
        slots_kernel,
        [
            jax.ShapeDtypeStruct((2, tok_rows), jnp.int32),
            jax.ShapeDtypeStruct((slots_all, tok_rows), BF16),
        ],
        routes.T,
    )
    outgoing = kernel(
        dispatch_kernel, jax.ShapeDtypeStruct((2, slots_all, width), BF16), dispatch, gathered
    )
    rows = exchanged(outgoing.reshape(4 * groups, few, width), ("zp", "core", "ep"))

    gain_pieces = gathered[:, part_width, : 3 * part_width].astype(F32)
    gain = gain_pieces.reshape(columns, 3, part_width).sum(axis=1).reshape(1, width)
    gain = lax.all_gather(gain, ("zp", "core"), axis=0, tiled=True)

    gate = expert_gate.reshape(columns, 4, part_width, units)
    up = expert_up.reshape(columns, 4, part_width, units)
    down = kernel(
        reorder_kernel,
        pltpu.HBM((4, units, width), BF16),
        in_hbm(expert_down.reshape(units, full_width)),
        in_specs=[HBM],
        out_specs=HBM,
        scratch_shapes=[
            pltpu.VMEM((units, full_width), BF16),
            pltpu.VMEM((4, units, width), BF16),
            pltpu.SemaphoreType.DMA((2,)),
        ],
    )
    gate_peer = swapped(gate)
    up_peer = swapped(up)
    down_peer = swapped(down)
    sent = kernel(
        expert_kernel,
        jax.ShapeDtypeStruct((4, groups * few, width), BF16),
        rows.reshape(4, groups * few, width),
        gain,
        *(in_hbm(w) for w in (gate, up, gate_peer, up_peer, down, down_peer)),
        in_specs=[VMEM] * 2 + [HBM] * 6,
        scratch_shapes=[
            pltpu.VMEM((2, 4, columns, part_width, units), BF16),
            pltpu.VMEM((2, 4, columns, part_width, units), BF16),
            pltpu.VMEM((2, 4, units, width), BF16),
            pltpu.VMEM((groups * few, full_width), BF16),
            pltpu.SemaphoreType.DMA((3, 2, 4)),
        ],
    )
    returned = exchanged(sent.reshape(4 * groups, few, width), ("zp", "core", "ep"))

    partial = kernel(
        combine_kernel,
        jax.ShapeDtypeStruct((width, tok_rows), BF16),
        returned.reshape(2, slots_all, width),
        places,
        route_weights.T,
    )
    parts = exchanged(partial.reshape(columns, part_width, tok_rows), "z8")
    combined = jnp.sum(parts.astype(F32), axis=0)
    own_sq = jnp.sum(combined * combined, axis=0)
    copies = jnp.broadcast_to(own_sq[None, None], (lax.axis_size(TP), 1, tok_rows))
    output_sq = jnp.sum(exchanged(copies, TP), axis=(0, 1))
    result = combined * lax.rsqrt(output_sq / full_width + EPSILON) * post_gain[:, None]
    return result.astype(BF16).T


def solution(mesh):
    torus = Mesh(mesh.devices.reshape(mesh.shape["ep"], 8, 2, 2), ("ep", *TP))
    in_specs = (
        P("ep", TP),
        P(TP),
        P("ep", None, TP),
        P("ep", None, TP),
        P("ep", TP, None),
        P("ep", None),
        P("ep", None),
        P(TP),
    )

    return jax.shard_map(
        local, mesh=torus, in_specs=in_specs, out_specs=P("ep", TP), check_vma=False
    )
```

time: 154 us -> 148 us (0.961)
  blocking collectives: 103 us -> 79.3 us
  starting transfers between devices: 24 us -> 35.2 us
  waiting for transfers between devices: 11 us -> 18.8 us
  Pallas kernels: 8.52 us -> 10.4 us
  matrix products: 1.78 us -> 0 us
    all_gather x1, blocking collectives: 32.1 us -> 10.8 us  [local(): gain = lax.all_gather(gain, ('zp', 'core'), axis=0, tiled=True)]
    all_to_all x1 -> x2, starting transfers between devices: 7.35 us -> 28.5 us  [exchanged(): return lax.all_to_all(value, axis, split_axis=0, concat_axis=0, tiled=True)]
    ppermute x4 -> x3, starting transfers between devices: 16.6 us -> 6.69 us  [swapped(): return lax.ppermute(value, 'core', [(0, 1), (1, 0)])]
    all_to_all x1 -> x2, waiting for transfers between devices: 10.3 us -> 18.8 us  [exchanged(): return lax.all_to_all(value, axis, split_axis=0, concat_axis=0, tiled=True)]
    all_to_all x3, blocking collectives: 71.2 us -> 68.5 us  [exchanged(): return lax.all_to_all(value, axis, split_axis=0, concat_axis=0, tiled=True)]
    pallas_call x4 -> x5, Pallas kernels: 8.52 us -> 10.4 us  [kernel(): pl.pallas_call(body, in_specs=in_specs or [VMEM] * len(operands), out_spe...]
    dot_general x1 -> x0, matrix products: 1.78 us -> none  [local(): lax.dot_general(dispatch, normed, (((1,), (1,)), ((), ())), preferred_ele...]
    unnamed x14 -> x10, local copies, waits for them, and re-layouts: 2.51 us -> 0.77 us
  transfers between devices with their start and end apart: 5 -> 5, of which waited for: 3 -> 2; matrix products, arithmetic and copies ran while one was open for 0% -> 0% of each run, Pallas kernels for 2% -> 2%
where the time goes in v4:
time: 148 us
  blocking collectives  79.3 us (54%)
  starting transfers between devices  35.2 us (24%)
  waiting for transfers between devices  18.8 us (13%)
  Pallas kernels  10.4 us (7%)
  other arithmetic  2.3 us (2%)
  local copies, waits for them, and re-layouts  1.69 us (1%)
    all_to_all x3, blocking collectives, exchanged(): return lax.all_to_all(value, axis, split_axis=0, concat_axis=0, tiled=True)  68.5 us
    all_to_all x2, starting transfers between devices, exchanged(): return lax.all_to_all(value, axis, split_axis=0, concat_axis=0, tiled=True)  28.5 us
    all_to_all x2, waiting for transfers between devices, exchanged(): return lax.all_to_all(value, axis, split_axis=0, concat_axis=0, tiled=True)  18.8 us
    all_gather x1, blocking collectives, local(): gain = lax.all_gather(gain, ('zp', 'core'), axis=0, tiled=True)  10.8 us
    pallas_call x5, Pallas kernels, kernel(): pl.pallas_call(body, in_specs=in_specs or [VMEM] * len(operands), out_spe...  10.4 us
    ppermute x3, starting transfers between devices, swapped(): return lax.ppermute(value, 'core', [(0, 1), (1, 0)])  6.69 us
  transfers between devices with their start and end apart: 5, of which 2 were waited for; matrix products, arithmetic and copies ran while one was open for 0% of the time, Pallas kernels for 2%

profile of v4, /device:TPU:1, one launch (start us, length us, event | category | flops | bytes accessed | tf_op | source)
XLA Modules:
  0.0 147.8 jit_solution(151944544339530273)
XLA Ops:
  0.0 0.7 fusion.4
  0.7 0.1 convert_element_type.34
  0.8 0.8 fusion.1
  1.5 0.7 broadcast_in_dim.4
  2.3 15.6 %all-to-all-start = ((bf16[8,72,256]{2,1,0:T(8,128)(2,1)}), bf16[8,72,256]{2,1,0:T(8,128)(2,1)S(1)}, u32[]{:S(2)}, u32[]{:S(2)}) async-start(bf16[8,72,256]{2,1,0:T(8,128)(2,1)} %broadcast_in_dim.4), calls=%async_computation | async-start | bytes 589824 | tf_op jit(solution)/shard_map/all_to_all | solution.py:19
  17.9 0.0 copy-start.1
  17.9 0.7 copy-done.1
  18.6 0.4 shard_map.82
  19.0 16.7 %all-to-all-done.gathered = bf16[8,72,256]{2,1,0:T(8,128)(2,1)S(1)} async-done(((bf16[8,72,256]{2,1,0:T(8,128)(2,1)}), bf16[8,72,256]{2,1,0:T(8,128)(2,1)S(1)}, u32[]{:S(2)}, u32[]{:S(2)}) %all-to-all-start) | async-done | bytes 294944 | tf_op jit(solution)/shard_map/all_to_all | solution.py:19
  35.6 1.6 %shard_map.83 = bf16[2,768,512]{2,1,0:T(8,128)(2,1)} custom-call(bf16[768,256]{1,0:T(8,128)(2,1)S(1)} %get-tuple-element.7.dispatch, bf16[8,72,256]{2,1,0:T(8,128)(2,1)S(1)} %all-to-all-done.gathered), custom_call_target="tpu_custom_call" | custom-call | tf_op jit(solution)/shard_map/pallas_call | solution.py:38
  37.2 12.9 %all-to-all-start.1 = ((bf16[64,24,512]{2,1,0:T(8,128)(2,1)}), bf16[64,24,512]{2,1,0:T(8,128)(2,1)S(1)}, u32[]{:S(2)}, u32[]{:S(2)}) async-start(bf16[64,24,512]{2,1,0:T(8,128)(2,1)} %bitcast.5), calls=%async_computation.1 | async-start | bytes 3145728 | tf_op jit(solution)/shard_map/all_to_all | solution.py:19
  50.1 0.0 copy-start.2
  50.1 3.0 %shard_map.84.down_own = bf16[4,256,512]{2,1,0:T(8,128)(2,1)} custom-call(bf16[256,2048]{1,0:T(8,128)(2,1)} %bitcast.29), custom_call_target="tpu_custom_call" | custom-call | tf_op jit(solution)/shard_map/pallas_call | solution.py:38
  53.1 2.4 %collective-permute-start.2 = (bf16[4,256,512]{2,1,0:T(8,128)(2,1)}, bf16[4,256,512]{2,1,0:T(8,128)(2,1)}, u32[]{:S(2)}, u32[]{:S(2)}) collective-permute-start(bf16[4,256,512]{2,1,0:T(8,128)(2,1)} %shard_map.84.down_own), channel_id=1, source_target_pairs={{0,1},{1,0},{2,3},{3,2},{4,5},{5,4},{6,7},{7,6},{8,9},{9,8},{10,11... | collective-permute-start | bytes 3145736 | tf_op jit(solution)/shard_map/ppermute | solution.py:23
  55.4 0.0 copy-done.2
  55.4 2.0 %collective-permute-start = (bf16[8,4,64,256]{3,2,1,0:T(8,128)(2,1)S(1)}, bf16[8,4,64,256]{3,2,1,0:T(8,128)(2,1)}, u32[]{:S(2)}, u32[]{:S(2)}) collective-permute-start(bf16[8,4,64,256]{3,2,1,0:T(8,128)(2,1)S(1)} %bitcast.31), channel_id=1, source_target_pairs={{0,1},{1,0},{2,3},{3,2},{4,5},{5,4},{6,7},{7,6},{8,9},{9,8},{10,11... | collective-permute-start | bytes 3145736 | tf_op jit(solution)/shard_map/ppermute | solution.py:23
  57.4 2.4 %collective-permute-start.1 = (bf16[8,4,64,256]{3,2,1,0:T(8,128)(2,1)}, bf16[8,4,64,256]{3,2,1,0:T(8,128)(2,1)}, u32[]{:S(2)}, u32[]{:S(2)}) collective-permute-start(bf16[8,4,64,256]{3,2,1,0:T(8,128)(2,1)} %bitcast.8.up_own), channel_id=1, source_target_pairs={{0,1},{1,0},{2,3},{3,2},{4,5},{5,4},{6,7},{7,6},{8,9},{9,8},{10,11... | collective-permute-start | bytes 3145736 | tf_op jit(solution)/shard_map/ppermute | solution.py:23
  59.8 0.1 reshape.61
  59.9 0.1 reshape.62
  60.0 10.8 %all-gather = f32[4,1,512]{2,1,0:T(1,128)S(1)} all-gather(f32[1,1,512]{2,1,0:T(1,128)S(1)} %reshape.62), channel_id=1, replica_groups=mesh['ep'=16,'z8'=8,'zp'=2,'core'=2] {'zp','core'}, dimensions={0}, use_global_device_ids=true | all-gather | bytes 10240 | tf_op jit(solution)/shard_map/all_gather | solution.py:208
  70.8 0.0 collective-permute-done.2.down_peer
  70.8 0.0 collective-permute-done.gate_peer
  70.8 0.0 collective-permute-done.1.up_peer
  70.8 2.1 %all-to-all-done.1 = bf16[64,24,512]{2,1,0:T(8,128)(2,1)S(1)} async-done(((bf16[64,24,512]{2,1,0:T(8,128)(2,1)}), bf16[64,24,512]{2,1,0:T(8,128)(2,1)S(1)}, u32[]{:S(2)}, u32[]{:S(2)}) %all-to-all-start.1) | async-done | bytes 1572896 | tf_op jit(solution)/shard_map/all_to_all | solution.py:19
  72.9 4.9 %shard_map.85 = bf16[4,384,512]{2,1,0:T(8,128)(2,1)S(1)} custom-call(bf16[4,384,512]{2,1,0:T(8,128)(2,1)S(1)} %bitcast.23, f32[4,512]{1,0:T(4,128)S(1)} %bitcast.26, bf16[8,4,64,256]{3,2,1,0:T(8,128)(2,1)} %bitcast.30, bf16[8,4,64,256]{3,2,1,0:T(8,128)(2,1)} %bitcast.8.up_own, bf16[8,4,64,256]{3,2,1,0:T(8,128)(2,1)} %collective-permute-done.gate_peer, ...), custom_call_target="tpu_custom_call" | custom-call | tf_op jit(solution)/shard_map/pallas_call | solution.py:38
  77.8 0.0 copy-start
  77.8 28.0 %all_to_all.25 = bf16[64,24,512]{2,1,0:T(8,128)(2,1)S(1)} all-to-all(bf16[64,24,512]{2,1,0:T(8,128)(2,1)S(1)} %bitcast.24), channel_id=1, replica_groups=mesh['ep'=16,'z8'=8,'zp'=2,'core'=2] {'zp','core','ep'}, dimensions={0} | all-to-all | bytes 3145728 | tf_op jit(solution)/shard_map/all_to_all | solution.py:19
  105.8 0.0 copy-start.3
  105.8 0.0 copy-done
  105.8 0.6 shard_map.86
  106.4 21.0 %all_to_all.26 = bf16[8,64,256]{2,1,0:T(8,128)(2,1)S(1)} all-to-all(bf16[8,64,256]{2,1,0:T(8,128)(2,1)S(1)} %bitcast.25), channel_id=1, replica_groups=mesh['ep'=16,'z8'=8,'zp'=2,'core'=2] {'z8'}, dimensions={0} | all-to-all | bytes 524288 | tf_op jit(solution)/shard_map/all_to_all | solution.py:19
  127.5 19.5 %all_to_all.27 = f32[32,1,256]{2,1,0:T(1,128)S(1)} all-to-all(f32[32,1,256]{2,1,0:T(1,128)S(1)} %broadcast_in_dim.5), channel_id=1, replica_groups=mesh['ep'=16,'z8'=8,'zp'=2,'core'=2] {'z8','zp','core'}, dimensions={0} | all-to-all | bytes 65536 | tf_op jit(solution)/shard_map/all_to_all | solution.py:19
  147.0 0.1 reduce_sum.39
  147.1 0.0 copy-done.3
  147.1 0.7 fusion.2
  (8 shorter events, 0.2 us)
Async XLA Ops:
  2.3 33.4 %all-to-all-start = ((bf16[8,72,256]{2,1,0:T(8,128)(2,1)}), bf16[8,72,256]{2,1,0:T(8,128)(2,1)S(1)}, u32[]{:S(2)}, u32[]{:S(2)}) async-start(bf16[8,72,256]{2,1,0:T(8,128)(2,1)} %broadcast_in_dim.4), calls=%async_computation | async-start | bytes 589824 | tf_op jit(solution)/shard_map/all_to_all | solution.py:19
  17.9 0.7 copy-start.1
  37.2 35.7 %all-to-all-start.1 = ((bf16[64,24,512]{2,1,0:T(8,128)(2,1)}), bf16[64,24,512]{2,1,0:T(8,128)(2,1)S(1)}, u32[]{:S(2)}, u32[]{:S(2)}) async-start(bf16[64,24,512]{2,1,0:T(8,128)(2,1)} %bitcast.5), calls=%async_computation.1 | async-start | bytes 3145728 | tf_op jit(solution)/shard_map/all_to_all | solution.py:19
  50.1 5.4 %copy-start.2 = (bf16[1,2048,256]{2,1,0:T(8,128)(2,1)S(1)}, bf16[1,2048,256]{2,1,0:T(8,128)(2,1)}, u32[]{:S(2)}) copy-start(bf16[1,2048,256]{2,1,0:T(8,128)(2,1)} %param.10) | copy-start | bytes 3145732
  53.1 17.8 %collective-permute-start.2 = (bf16[4,256,512]{2,1,0:T(8,128)(2,1)}, bf16[4,256,512]{2,1,0:T(8,128)(2,1)}, u32[]{:S(2)}, u32[]{:S(2)}) collective-permute-start(bf16[4,256,512]{2,1,0:T(8,128)(2,1)} %shard_map.84.down_own), channel_id=1, source_target_pairs={{0,1},{1,0},{2,3},{3,2},{4,5},{5,4},{6,7},{7,6},{8,9},{9,8},{10,11... | collective-permute-start | bytes 3145736 | tf_op jit(solution)/shard_map/ppermute | solution.py:23
  55.4 15.4 %collective-permute-start = (bf16[8,4,64,256]{3,2,1,0:T(8,128)(2,1)S(1)}, bf16[8,4,64,256]{3,2,1,0:T(8,128)(2,1)}, u32[]{:S(2)}, u32[]{:S(2)}) collective-permute-start(bf16[8,4,64,256]{3,2,1,0:T(8,128)(2,1)S(1)} %bitcast.31), channel_id=1, source_target_pairs={{0,1},{1,0},{2,3},{3,2},{4,5},{5,4},{6,7},{7,6},{8,9},{9,8},{10,11... | collective-permute-start | bytes 3145736 | tf_op jit(solution)/shard_map/ppermute | solution.py:23
  57.4 13.4 %collective-permute-start.1 = (bf16[8,4,64,256]{3,2,1,0:T(8,128)(2,1)}, bf16[8,4,64,256]{3,2,1,0:T(8,128)(2,1)}, u32[]{:S(2)}, u32[]{:S(2)}) collective-permute-start(bf16[8,4,64,256]{3,2,1,0:T(8,128)(2,1)} %bitcast.8.up_own), channel_id=1, source_target_pairs={{0,1},{1,0},{2,3},{3,2},{4,5},{5,4},{6,7},{7,6},{8,9},{9,8},{10,11... | collective-permute-start | bytes 3145736 | tf_op jit(solution)/shard_map/ppermute | solution.py:23
  77.8 28.0 %copy-start = (f32[256,2]{0,1:T(2,128)S(1)}, f32[256,2]{0,1:T(2,128)}, u32[]{:S(2)}) copy-start(f32[256,2]{0,1:T(2,128)} %param.14) | copy-start | bytes 6148
  105.8 41.3 %copy-start.3 = (f32[64]{0:T(128)S(1)}, f32[64]{0:T(128)}, u32[]{:S(2)}) copy-start(f32[64]{0:T(128)} %param.15) | copy-start | bytes 772

commit v5 on v4

--- a/solution.py
+++ b/solution.py
@@ -13,6 +13,7 @@
 MIB = 1024 * 1024
 VMEM = pl.BlockSpec(memory_space=pltpu.VMEM)
 HBM = pl.BlockSpec(memory_space=pltpu.HBM)
+ANY = pl.BlockSpec(memory_space=pl.ANY)
 
 
 def exchanged(value, axis):
@@ -21,13 +22,6 @@
 
 def swapped(value):
     return lax.ppermute(value, "core", [(0, 1), (1, 0)])
-
-
-def three_pieces(value):
-    high = lax.reduce_precision(value, 8, 7)
-    middle = lax.reduce_precision(value - high, 8, 7)
-    low = lax.reduce_precision(value - high - middle, 8, 7)
-    return jnp.stack([high, middle, low]).astype(BF16)
 
 
 def in_hbm(value):
@@ -43,6 +37,26 @@
         scratch_shapes=scratch_shapes,
         compiler_params=pltpu.CompilerParams(vmem_limit_bytes=16 * MIB),
     )(*operands)
+
+
+def spread_kernel(tokens, gain, copies, payload, sems):
+    part_width, lanes = tokens.shape[0], payload.shape[1]
+    payload[0:part_width, :] = tokens[:, :lanes]
+    payload[part_width : 2 * part_width, :] = tokens[:, lanes:]
+    value = gain[...]
+    high = value.astype(BF16).astype(F32)
+    middle = (value - high).astype(BF16).astype(F32)
+    low = value - high - middle
+    row = lax.broadcasted_iota(jnp.int32, (8, lanes), 0)
+    picked = jnp.where(row == 0, high, jnp.where(row == 1, middle, jnp.where(row == 2, low, 0.0)))
+    payload[2 * part_width :, :] = picked.astype(BF16)
+    leaving = [
+        pltpu.make_async_copy(payload, copies.at[k], sems.at[k]) for k in range(copies.shape[0])
+    ]
+    for copy in leaving:
+        copy.start()
+    for copy in leaving:
+        copy.wait()
 
 
 def slots_kernel(chosen, places, dispatch):
@@ -70,15 +84,27 @@
     dispatch[...] = taken.astype(F32).astype(BF16)
 
 
-def dispatch_kernel(dispatch, gathered, outgoing):
+def dispatch_kernel(dispatch, gathered, outgoing, held, sems):
     part_width = 64
-    columns, _, tok_rows = gathered.shape
-    features = gathered[:, :part_width, :].reshape(columns * part_width, tok_rows)
-    value = lax.dot_general(
-        dispatch[...], features, (((1,), (1,)), ((), ())), preferred_element_type=F32
-    ).astype(BF16)
-    outgoing[0] = value
-    outgoing[1] = value
+    lower = gathered[:, :part_width, :]
+    upper = gathered[:, part_width : 2 * part_width, :]
+    features = jnp.concatenate([lower, upper], axis=2).reshape(-1, 2 * gathered.shape[2])
+    length = dispatch.shape[0]
+    step = length // 4
+    leaving = []
+    for k in range(4):
+        here = pl.ds(k * step, step)
+        held[here, :] = lax.dot_general(
+            dispatch[here, :], features, (((1,), (1,)), ((), ())), preferred_element_type=F32
+        ).astype(BF16)
+        for pair in range(2):
+            copy = pltpu.make_async_copy(
+                held.at[here], outgoing.at[pair, here], sems.at[pair, k]
+            )
+            copy.start()
+            leaving.append(copy)
+    for copy in leaving:
+        copy.wait()
 
 
 def reorder_kernel(down, split_down, held, turned, sems):
@@ -185,9 +211,18 @@
     slots_all = 2 * groups * few
     units = expert_gate.shape[-1]
 
-    pieces = jnp.pad(three_pieces(pre_gain).reshape(1, -1), ((0, 7), (0, tok_rows - 3 * part_width)))
-    payload = jnp.concatenate([tokens.T, pieces], axis=0)
-    copies = jnp.broadcast_to(payload, (columns, *payload.shape))
+    lanes = tok_rows // 2
+    copies = kernel(
+        spread_kernel,
+        pltpu.HBM((columns, 2 * part_width + 8, lanes), BF16),
+        tokens.T,
+        jnp.pad(pre_gain[None], ((0, 0), (0, lanes - part_width))),
+        out_specs=HBM,
+        scratch_shapes=[
+            pltpu.VMEM((2 * part_width + 8, lanes), BF16),
+            pltpu.SemaphoreType.DMA((columns,)),
+        ],
+    )
     gathered = exchanged(copies, "z8")
 
     places, dispatch = kernel(
@@ -199,12 +234,17 @@
         routes.T,
     )
     outgoing = kernel(
-        dispatch_kernel, jax.ShapeDtypeStruct((2, slots_all, width), BF16), dispatch, gathered
+        dispatch_kernel,
+        pltpu.HBM((2, slots_all, width), BF16),
+        dispatch,
+        gathered,
+        out_specs=HBM,
+        scratch_shapes=[pltpu.VMEM((slots_all, width), BF16), pltpu.SemaphoreType.DMA((2, 4))],
     )
     rows = exchanged(outgoing.reshape(4 * groups, few, width), ("zp", "core", "ep"))
 
-    gain_pieces = gathered[:, part_width, : 3 * part_width].astype(F32)
-    gain = gain_pieces.reshape(columns, 3, part_width).sum(axis=1).reshape(1, width)
+    gain = gathered[:, 2 * part_width : 2 * part_width + 3, :part_width].astype(F32)
+    gain = gain.sum(axis=1).reshape(1, width)
     gain = lax.all_gather(gain, ("zp", "core"), axis=0, tiled=True)
 
     gate = expert_gate.reshape(columns, 4, part_width, units)
@@ -229,8 +269,13 @@
         jax.ShapeDtypeStruct((4, groups * few, width), BF16),
         rows.reshape(4, groups * few, width),
         gain,
-        *(in_hbm(w) for w in (gate, up, gate_peer, up_peer, down, down_peer)),
-        in_specs=[VMEM] * 2 + [HBM] * 6,
+        in_hbm(gate),
+        in_hbm(up),
+        gate_peer,
+        in_hbm(up_peer),
+        in_hbm(down),
+        in_hbm(down_peer),
+        in_specs=[VMEM] * 2 + [HBM] * 2 + [ANY] + [HBM] * 3,
         scratch_shapes=[
             pltpu.VMEM((2, 4, columns, part_width, units), BF16),
             pltpu.VMEM((2, 4, columns, part_width, units), BF16),

time: 148 us -> 148 us (level)
    pallas_call x5 -> x6, Pallas kernels: 10.4 us -> 11 us  [kernel(): pl.pallas_call(body, in_specs=in_specs or [VMEM] * len(operands), out_spe...]
where the time goes in v5:
time: 148 us; the launch traced here: 147 us
  blocking collectives  79.2 us (54%)
  starting transfers between devices  35 us (24%)
  waiting for transfers between devices  18.5 us (12%)
  Pallas kernels  11 us (7%)
  local copies, waits for them, and re-layouts  2.2 us (1%)
    all_to_all x3, blocking collectives, exchanged(): return lax.all_to_all(value, axis, split_axis=0, concat_axis=0, tiled=True)  68.2 us
    all_to_all x2, starting transfers between devices, exchanged(): return lax.all_to_all(value, axis, split_axis=0, concat_axis=0, tiled=True)  28.3 us
    all_to_all x2, waiting for transfers between devices, exchanged(): return lax.all_to_all(value, axis, split_axis=0, concat_axis=0, tiled=True)  18.5 us
    pallas_call x6, Pallas kernels, kernel(): pl.pallas_call(body, in_specs=in_specs or [VMEM] * len(operands), out_spe...  11 us
    all_gather x1, blocking collectives, local(): gain = lax.all_gather(gain, ('zp', 'core'), axis=0, tiled=True)  11 us
    ppermute x3, starting transfers between devices, swapped(): return lax.ppermute(value, 'core', [(0, 1), (1, 0)])  6.69 us
  transfers between devices with their start and end apart: 5, of which 2 were waited for; matrix products, arithmetic and copies ran while one was open for 0% of the time, Pallas kernels for 2%

profile of v5, /device:TPU:1, one launch (start us, length us, event | category | flops | bytes accessed | tf_op | source)
XLA Modules:
  0.0 146.9 jit_solution(1451425983751269596)
XLA Ops:
  0.0 0.7 pad.4.gain
  0.7 0.0 copy-start
  0.7 0.8 copy-done
  1.4 0.8 shard_map.83
  2.2 15.6 %all-to-all-start = ((bf16[8,136,128]{2,1,0:T(8,128)(2,1)}), bf16[8,136,128]{2,1,0:T(8,128)(2,1)S(1)}, u32[]{:S(2)}, u32[]{:S(2)}) async-start(bf16[8,136,128]{2,1,0:T(8,128)(2,1)} %shard_map.83), calls=%async_computation | async-start | bytes 557056 | tf_op jit(solution)/shard_map/all_to_all | solution.py:20
  17.9 0.0 copy-start.2
  17.9 0.7 copy-done.2
  18.5 0.4 shard_map.82
  18.9 16.4 %all-to-all-done.gathered = bf16[8,136,128]{2,1,0:T(8,128)(2,1)S(1)} async-done(((bf16[8,136,128]{2,1,0:T(8,128)(2,1)}), bf16[8,136,128]{2,1,0:T(8,128)(2,1)S(1)}, u32[]{:S(2)}, u32[]{:S(2)}) %all-to-all-start) | async-done | bytes 278560 | tf_op jit(solution)/shard_map/all_to_all | solution.py:20
  35.4 1.5 %shard_map.84 = bf16[2,768,512]{2,1,0:T(8,128)(2,1)} custom-call(bf16[768,256]{1,0:T(8,128)(2,1)S(1)} %get-tuple-element.7.dispatch, bf16[8,136,128]{2,1,0:T(8,128)(2,1)S(1)} %all-to-all-done.gathered), custom_call_target="tpu_custom_call" | custom-call | tf_op jit(solution)/shard_map/pallas_call | solution.py:32
  36.9 12.7 %all-to-all-start.1 = ((bf16[64,24,512]{2,1,0:T(8,128)(2,1)}), bf16[64,24,512]{2,1,0:T(8,128)(2,1)S(1)}, u32[]{:S(2)}, u32[]{:S(2)}) async-start(bf16[64,24,512]{2,1,0:T(8,128)(2,1)} %bitcast.25), calls=%async_computation.1 | async-start | bytes 3145728 | tf_op jit(solution)/shard_map/all_to_all | solution.py:20
  49.6 2.9 %shard_map.85.down_own = bf16[4,256,512]{2,1,0:T(8,128)(2,1)} custom-call(bf16[256,2048]{1,0:T(8,128)(2,1)} %bitcast.26), custom_call_target="tpu_custom_call" | custom-call | tf_op jit(solution)/shard_map/pallas_call | solution.py:32
  52.5 2.4 %collective-permute-start.2 = (bf16[4,256,512]{2,1,0:T(8,128)(2,1)}, bf16[4,256,512]{2,1,0:T(8,128)(2,1)}, u32[]{:S(2)}, u32[]{:S(2)}) collective-permute-start(bf16[4,256,512]{2,1,0:T(8,128)(2,1)} %shard_map.85.down_own), channel_id=1, source_target_pairs={{0,1},{1,0},{2,3},{3,2},{4,5},{5,4},{6,7},{7,6},{8,9},{9,8},{10,11... | collective-permute-start | bytes 3145736 | tf_op jit(solution)/shard_map/ppermute | solution.py:24
  54.9 2.0 %collective-permute-start = (bf16[8,4,64,256]{3,2,1,0:T(8,128)(2,1)}, bf16[8,4,64,256]{3,2,1,0:T(8,128)(2,1)S(1)}, u32[]{:S(2)}, u32[]{:S(2)}) collective-permute-start(bf16[8,4,64,256]{3,2,1,0:T(8,128)(2,1)} %bitcast.5.gate_own), channel_id=1, source_target_pairs={{0,1},{1,0},{2,3},{3,2},{4,5},{5,4},{6,7},{7,6},{8,9},{9,8},{10,11... | collective-permute-start | bytes 3145736 | tf_op jit(solution)/shard_map/ppermute | solution.py:24
  56.9 2.4 %collective-permute-start.1 = (bf16[8,4,64,256]{3,2,1,0:T(8,128)(2,1)}, bf16[8,4,64,256]{3,2,1,0:T(8,128)(2,1)}, u32[]{:S(2)}, u32[]{:S(2)}) collective-permute-start(bf16[8,4,64,256]{3,2,1,0:T(8,128)(2,1)} %bitcast.6.up_own), channel_id=1, source_target_pairs={{0,1},{1,0},{2,3},{3,2},{4,5},{5,4},{6,7},{7,6},{8,9},{9,8},{10,11... | collective-permute-start | bytes 3145736 | tf_op jit(solution)/shard_map/ppermute | solution.py:24
  59.2 0.1 reshape.45
  59.3 11.0 %all-gather = f32[4,1,512]{2,1,0:T(1,128)S(1)} all-gather(f32[1,1,512]{2,1,0:T(1,128)S(1)} %reshape.45), channel_id=1, replica_groups=mesh['ep'=16,'z8'=8,'zp'=2,'core'=2] {'zp','core'}, dimensions={0}, use_global_device_ids=true | all-gather | bytes 10240 | tf_op jit(solution)/shard_map/all_gather | solution.py:248
  70.3 0.0 collective-permute-done.2.down_peer
  70.3 0.0 collective-permute-done.gate_peer
  70.3 0.0 collective-permute-done.1.up_peer
  70.3 2.1 %all-to-all-done.1 = bf16[64,24,512]{2,1,0:T(8,128)(2,1)S(1)} async-done(((bf16[64,24,512]{2,1,0:T(8,128)(2,1)}), bf16[64,24,512]{2,1,0:T(8,128)(2,1)S(1)}, u32[]{:S(2)}, u32[]{:S(2)}) %all-to-all-start.1) | async-done | bytes 1572896 | tf_op jit(solution)/shard_map/all_to_all | solution.py:20
  72.4 4.8 %shard_map.86 = bf16[4,384,512]{2,1,0:T(8,128)(2,1)S(1)} custom-call(bf16[4,384,512]{2,1,0:T(8,128)(2,1)S(1)} %bitcast.18, f32[4,512]{1,0:T(4,128)S(1)} %bitcast.22, bf16[8,4,64,256]{3,2,1,0:T(8,128)(2,1)} %bitcast.5.gate_own, bf16[8,4,64,256]{3,2,1,0:T(8,128)(2,1)} %bitcast.6.up_own, bf16[8,4,64,256]{3,2,1,0:T(8,128)(2,1)S(1)} %collective-permute-done.gate_peer, ...), custom_call_target="tpu_custom_call" | custom-call | tf_op jit(solution)/shard_map/pallas_call | solution.py:32
  77.2 0.0 copy-start.1
  77.2 28.0 %all_to_all.25 = bf16[64,24,512]{2,1,0:T(8,128)(2,1)S(1)} all-to-all(bf16[64,24,512]{2,1,0:T(8,128)(2,1)S(1)} %bitcast.19), channel_id=1, replica_groups=mesh['ep'=16,'z8'=8,'zp'=2,'core'=2] {'zp','core','ep'}, dimensions={0} | all-to-all | bytes 3145728 | tf_op jit(solution)/shard_map/all_to_all | solution.py:20
  105.2 0.0 copy-start.3
  105.2 0.0 copy-done.1
  105.2 0.6 shard_map.87
  105.8 20.7 %all_to_all.26 = bf16[8,64,256]{2,1,0:T(8,128)(2,1)S(1)} all-to-all(bf16[8,64,256]{2,1,0:T(8,128)(2,1)S(1)} %bitcast.20), channel_id=1, replica_groups=mesh['ep'=16,'z8'=8,'zp'=2,'core'=2] {'z8'}, dimensions={0} | all-to-all | bytes 524288 | tf_op jit(solution)/shard_map/all_to_all | solution.py:20
  126.6 19.5 %all_to_all.27 = f32[32,1,256]{2,1,0:T(1,128)S(1)} all-to-all(f32[32,1,256]{2,1,0:T(1,128)S(1)} %broadcast_in_dim.5), channel_id=1, replica_groups=mesh['ep'=16,'z8'=8,'zp'=2,'core'=2] {'z8','zp','core'}, dimensions={0} | all-to-all | bytes 65536 | tf_op jit(solution)/shard_map/all_to_all | solution.py:20
  146.1 0.1 reduce_sum.39
  146.2 0.0 copy-done.3
  146.2 0.7 fusion
  (6 shorter events, 0.1 us)
Async XLA Ops:
  0.7 0.8 copy-start
  2.2 33.2 %all-to-all-start = ((bf16[8,136,128]{2,1,0:T(8,128)(2,1)}), bf16[8,136,128]{2,1,0:T(8,128)(2,1)S(1)}, u32[]{:S(2)}, u32[]{:S(2)}) async-start(bf16[8,136,128]{2,1,0:T(8,128)(2,1)} %shard_map.83), calls=%async_computation | async-start | bytes 557056 | tf_op jit(solution)/shard_map/all_to_all | solution.py:20
  17.9 0.7 copy-start.2
  36.9 35.5 %all-to-all-start.1 = ((bf16[64,24,512]{2,1,0:T(8,128)(2,1)}), bf16[64,24,512]{2,1,0:T(8,128)(2,1)S(1)}, u32[]{:S(2)}, u32[]{:S(2)}) async-start(bf16[64,24,512]{2,1,0:T(8,128)(2,1)} %bitcast.25), calls=%async_computation.1 | async-start | bytes 3145728 | tf_op jit(solution)/shard_map/all_to_all | solution.py:20
  52.5 17.8 %collective-permute-start.2 = (bf16[4,256,512]{2,1,0:T(8,128)(2,1)}, bf16[4,256,512]{2,1,0:T(8,128)(2,1)}, u32[]{:S(2)}, u32[]{:S(2)}) collective-permute-start(bf16[4,256,512]{2,1,0:T(8,128)(2,1)} %shard_map.85.down_own), channel_id=1, source_target_pairs={{0,1},{1,0},{2,3},{3,2},{4,5},{5,4},{6,7},{7,6},{8,9},{9,8},{10,11... | collective-permute-start | bytes 3145736 | tf_op jit(solution)/shard_map/ppermute | solution.py:24
  54.9 15.5 %collective-permute-start = (bf16[8,4,64,256]{3,2,1,0:T(8,128)(2,1)}, bf16[8,4,64,256]{3,2,1,0:T(8,128)(2,1)S(1)}, u32[]{:S(2)}, u32[]{:S(2)}) collective-permute-start(bf16[8,4,64,256]{3,2,1,0:T(8,128)(2,1)} %bitcast.5.gate_own), channel_id=1, source_target_pairs={{0,1},{1,0},{2,3},{3,2},{4,5},{5,4},{6,7},{7,6},{8,9},{9,8},{10,11... | collective-permute-start | bytes 3145736 | tf_op jit(solution)/shard_map/ppermute | solution.py:24
  56.9 13.5 %collective-permute-start.1 = (bf16[8,4,64,256]{3,2,1,0:T(8,128)(2,1)}, bf16[8,4,64,256]{3,2,1,0:T(8,128)(2,1)}, u32[]{:S(2)}, u32[]{:S(2)}) collective-permute-start(bf16[8,4,64,256]{3,2,1,0:T(8,128)(2,1)} %bitcast.6.up_own), channel_id=1, source_target_pairs={{0,1},{1,0},{2,3},{3,2},{4,5},{5,4},{6,7},{7,6},{8,9},{9,8},{10,11... | collective-permute-start | bytes 3145736 | tf_op jit(solution)/shard_map/ppermute | solution.py:24
  77.2 28.0 %copy-start.1 = (f32[256,2]{0,1:T(2,128)S(1)}, f32[256,2]{0,1:T(2,128)}, u32[]{:S(2)}) copy-start(f32[256,2]{0,1:T(2,128)} %param.14) | copy-start | bytes 6148
  105.2 41.0 %copy-start.3 = (f32[64]{0:T(128)S(1)}, f32[64]{0:T(128)}, u32[]{:S(2)}) copy-start(f32[64]{0:T(128)} %param.15) | copy-start | bytes 772

commit v6 on v5

--- a/solution.py
+++ b/solution.py
@@ -39,27 +39,34 @@
     )(*operands)
 
 
-def spread_kernel(tokens, gain, copies, payload, sems):
+def spread_kernel(
+    tokens_hbm, gain_hbm, chosen_hbm, copies, places, dispatch, tokens, gain, chosen, payload, in_sems
+):
+    coming = [
+        pltpu.make_async_copy(tokens_hbm, tokens, in_sems.at[0]),
+        pltpu.make_async_copy(gain_hbm, gain, in_sems.at[1]),
+        pltpu.make_async_copy(chosen_hbm, chosen, in_sems.at[2]),
+    ]
+    for copy in coming:
+        copy.start()
+    for copy in coming:
+        copy.wait()
     part_width, lanes = tokens.shape[0], payload.shape[1]
     payload[0:part_width, :] = tokens[:, :lanes]
     payload[part_width : 2 * part_width, :] = tokens[:, lanes:]
-    value = gain[...]
+    value = jnp.concatenate([gain[...], jnp.zeros_like(gain)], axis=1)
     high = value.astype(BF16).astype(F32)
     middle = (value - high).astype(BF16).astype(F32)
     low = value - high - middle
     row = lax.broadcasted_iota(jnp.int32, (8, lanes), 0)
     picked = jnp.where(row == 0, high, jnp.where(row == 1, middle, jnp.where(row == 2, low, 0.0)))
     payload[2 * part_width :, :] = picked.astype(BF16)
-    leaving = [
-        pltpu.make_async_copy(payload, copies.at[k], sems.at[k]) for k in range(copies.shape[0])
-    ]
-    for copy in leaving:
-        copy.start()
-    for copy in leaving:
-        copy.wait()
-
-
-def slots_kernel(chosen, places, dispatch):
+    for k in range(copies.shape[0]):
+        copies[k] = payload[...]
+    number_slots(chosen, places, dispatch)
+
+
+def number_slots(chosen, places, dispatch):
     slots_all, tok_rows = dispatch.shape
     groups = 16
     few = slots_all // groups // 2
@@ -88,14 +95,17 @@
     part_width = 64
     lower = gathered[:, :part_width, :]
     upper = gathered[:, part_width : 2 * part_width, :]
-    features = jnp.concatenate([lower, upper], axis=2).reshape(-1, 2 * gathered.shape[2])
+    width = gathered.shape[0] * part_width
+    lower = lower.reshape(width, -1).astype(F32).T.astype(BF16)
+    upper = upper.reshape(width, -1).astype(F32).T.astype(BF16)
+    features = jnp.concatenate([lower, upper], axis=0)
     length = dispatch.shape[0]
     step = length // 4
     leaving = []
     for k in range(4):
         here = pl.ds(k * step, step)
-        held[here, :] = lax.dot_general(
-            dispatch[here, :], features, (((1,), (1,)), ((), ())), preferred_element_type=F32
+        held[here, :] = jnp.dot(
+            dispatch[here, :], features, preferred_element_type=F32
         ).astype(BF16)
         for pair in range(2):
             copy = pltpu.make_async_copy(
@@ -133,26 +143,38 @@
 def expert_kernel(
     rows, gain, gate_own, up_own, gate_peer, up_peer, down_own, down_peer, sent, *scratch
 ):
-    gates, ups, downs, scaled, sems = scratch
+    held_up_peer, held_gate, held_up, down_first, down_second, scaled, sems = scratch
     parts, length, width = rows.shape
     units = gate_own.shape[-1]
-    copies = [[], [], []]
-    for stage, pairs in enumerate(((gate_own, up_own), (gate_peer, up_peer))):
-        for k, (source, target) in enumerate(zip(pairs, (gates, ups))):
-            for part in range(parts):
-                copies[stage].append(
-                    pltpu.make_async_copy(
-                        source.at[:, part], target.at[stage, part], sems.at[stage, k, part]
-                    )
-                )
-    for k, source in enumerate((down_own, down_peer)):
-        copies[2].append(pltpu.make_async_copy(source, downs.at[k], sems.at[2, k, 0]))
-    for stage in copies:
-        for copy in stage:
-            copy.start()
+    copies = [
+        pltpu.make_async_copy(source, target, sems.at[k])
+        for k, (source, target) in enumerate(
+            (
+                (up_peer, held_up_peer),
+                (gate_own, held_gate),
+                (up_own, held_up),
+                (down_peer, down_first),
+                (down_own, down_second),
+            )
+        )
+    ]
+    for copy in copies:
+        copy.start()
     step = 192
     starts = range(0, length, step)
+
+    def product(start, weight):
+        total = None
+        for part in range(parts):
+            value = scaled[start : start + step, part * width : (part + 1) * width]
+            more = jnp.dot(
+                value, weight[:, part].reshape(width, units), preferred_element_type=F32
+            )
+            total = more if total is None else total + more
+        return total * row_scale[start]
+
     row_scale = {}
+    gate_pre = {}
     for start in starts:
         here = slice(start, start + step)
         square = None
@@ -165,24 +187,28 @@
             ).astype(BF16)
         mean = jnp.sum(square, axis=1, keepdims=True) / (parts * width)
         row_scale[start] = lax.rsqrt(mean + EPSILON)
+        gate_pre[start] = product(start, gate_peer)
     hidden = {}
-    for which in range(2):
-        for copy in copies[which]:
-            copy.wait()
-        gate = gates[which].reshape(parts * width, units)
-        up = ups[which].reshape(parts * width, units)
-        for start in starts:
-            value = scaled[start : start + step, :]
-            gate_pre = jnp.dot(value, gate, preferred_element_type=F32) * row_scale[start]
-            up_pre = jnp.dot(value, up, preferred_element_type=F32) * row_scale[start]
-            hidden[which, start] = (gate_pre / (1.0 + jnp.exp(-gate_pre)) * up_pre).astype(BF16)
-    for copy in copies[2]:
-        copy.wait()
+    copies[0].wait()
+    for start in starts:
+        value = gate_pre[start]
+        up_pre = product(start, held_up_peer)
+        hidden[0, start] = (value / (1.0 + jnp.exp(-value)) * up_pre).astype(BF16)
+    copies[1].wait()
+    for start in starts:
+        gate_pre[start] = product(start, held_gate)
+    copies[2].wait()
+    for start in starts:
+        value = gate_pre[start]
+        up_pre = product(start, held_up)
+        hidden[1, start] = (value / (1.0 + jnp.exp(-value)) * up_pre).astype(BF16)
+    copies[3].wait()
+    copies[4].wait()
     for start in starts:
         here = slice(start, start + step)
         for part in range(parts):
-            out = jnp.dot(hidden[0, start], downs[0, part], preferred_element_type=F32)
-            out = out + jnp.dot(hidden[1, start], downs[1, part], preferred_element_type=F32)
+            out = jnp.dot(hidden[0, start], down_first[part], preferred_element_type=F32)
+            out = out + jnp.dot(hidden[1, start], down_second[part], preferred_element_type=F32)
             sent[part, here, :] = out.astype(BF16)
 
 
@@ -212,27 +238,27 @@
     units = expert_gate.shape[-1]
 
     lanes = tok_rows // 2
-    copies = kernel(
+    copies, places, dispatch = kernel(
         spread_kernel,
-        pltpu.HBM((columns, 2 * part_width + 8, lanes), BF16),
-        tokens.T,
-        jnp.pad(pre_gain[None], ((0, 0), (0, lanes - part_width))),
-        out_specs=HBM,
-        scratch_shapes=[
-            pltpu.VMEM((2 * part_width + 8, lanes), BF16),
-            pltpu.SemaphoreType.DMA((columns,)),
-        ],
-    )
-    gathered = exchanged(copies, "z8")
-
-    places, dispatch = kernel(
-        slots_kernel,
         [
+            jax.ShapeDtypeStruct((columns, 2 * part_width + 8, lanes), BF16),
             jax.ShapeDtypeStruct((2, tok_rows), jnp.int32),
             jax.ShapeDtypeStruct((slots_all, tok_rows), BF16),
         ],
-        routes.T,
-    )
+        in_hbm(tokens.T),
+        in_hbm(pre_gain[None]),
+        in_hbm(routes.T),
+        in_specs=[HBM] * 3,
+        scratch_shapes=[
+            pltpu.VMEM((part_width, tok_rows), BF16),
+            pltpu.VMEM((1, part_width), F32),
+            pltpu.VMEM((2, tok_rows), jnp.int32),
+            pltpu.VMEM((2 * part_width + 8, lanes), BF16),
+            pltpu.SemaphoreType.DMA((3,)),
+        ],
+    )
+    gathered = exchanged(copies, "z8")
+
     outgoing = kernel(
         dispatch_kernel,
         pltpu.HBM((2, slots_all, width), BF16),
@@ -275,14 +301,10 @@
         in_hbm(up_peer),
         in_hbm(down),
         in_hbm(down_peer),
-        in_specs=[VMEM] * 2 + [HBM] * 2 + [ANY] + [HBM] * 3,
-        scratch_shapes=[
-            pltpu.VMEM((2, 4, columns, part_width, units), BF16),
-            pltpu.VMEM((2, 4, columns, part_width, units), BF16),
-            pltpu.VMEM((2, 4, units, width), BF16),
-            pltpu.VMEM((groups * few, full_width), BF16),
-            pltpu.SemaphoreType.DMA((3, 2, 4)),
-        ],
+        in_specs=[VMEM] * 2 + [HBM] * 2 + [VMEM] + [HBM] * 3,
+        scratch_shapes=[pltpu.VMEM(gate.shape, BF16)] * 3
+        + [pltpu.VMEM(down.shape, BF16)] * 2
+        + [pltpu.VMEM((groups * few, full_width), BF16), pltpu.SemaphoreType.DMA((5,))],
     )
     returned = exchanged(sent.reshape(4 * groups, few, width), ("zp", "core", "ep"))
 

time: 148 us -> 146 us (0.986)
  blocking collectives: 79.2 us -> 111 us
  waiting for transfers between devices: 18.5 us -> 2.08 us
  starting transfers between devices: 35 us -> 20.1 us
  local copies, waits for them, and re-layouts: 2.2 us -> 0.11 us
    all_to_all x3 -> x4, blocking collectives: 68.2 us -> 100 us  [exchanged(): return lax.all_to_all(value, axis, split_axis=0, concat_axis=0, tiled=True)]
    all_to_all x2 -> x1, waiting for transfers between devices: 18.5 us -> 2.07 us  [exchanged(): return lax.all_to_all(value, axis, split_axis=0, concat_axis=0, tiled=True)]
    all_to_all x2 -> x1, starting transfers between devices: 28.3 us -> 13.4 us  [exchanged(): return lax.all_to_all(value, axis, split_axis=0, concat_axis=0, tiled=True)]
    pallas_call x6 -> x5, Pallas kernels: 11 us -> 10.9 us  [kernel(): pl.pallas_call(body, in_specs=in_specs or [VMEM] * len(operands), out_spe...]
  transfers between devices with their start and end apart: 5 -> 4, of which waited for: 2 -> 1; matrix products, arithmetic and copies ran while one was open for 0% -> 0% of each run, Pallas kernels for 2% -> 2%
where the time goes in v6:
time: 146 us
  blocking collectives  111 us (76%)
  starting transfers between devices  20.1 us (14%)
  Pallas kernels  10.9 us (7%)
  waiting for transfers between devices  2.08 us (1%)
    all_to_all x4, blocking collectives, exchanged(): return lax.all_to_all(value, axis, split_axis=0, concat_axis=0, tiled=True)  100 us
    all_to_all x1, starting transfers between devices, exchanged(): return lax.all_to_all(value, axis, split_axis=0, concat_axis=0, tiled=True)  13.4 us
    all_gather x1, blocking collectives, local(): gain = lax.all_gather(gain, ('zp', 'core'), axis=0, tiled=True)  11 us
    pallas_call x5, Pallas kernels, kernel(): pl.pallas_call(body, in_specs=in_specs or [VMEM] * len(operands), out_spe...  10.9 us
    ppermute x3, starting transfers between devices, swapped(): return lax.ppermute(value, 'core', [(0, 1), (1, 0)])  6.69 us
  transfers between devices with their start and end apart: 4, of which 1 were waited for; matrix products, arithmetic and copies ran while one was open for 0% of the time, Pallas kernels for 2%

profile of v6, /device:TPU:1, one launch (start us, length us, event | category | flops | bytes accessed | tf_op | source)
XLA Modules:
  0.0 145.6 jit_solution(13307310188701457176)
XLA Ops:
  0.0 1.2 shard_map.82
  1.2 32.8 %all_to_all.25.gathered = bf16[8,136,128]{2,1,0:T(8,128)(2,1)S(1)} all-to-all(bf16[8,136,128]{2,1,0:T(8,128)(2,1)S(1)} %get-tuple-element.9), channel_id=1, replica_groups=mesh['ep'=16,'z8'=8,'zp'=2,'core'=2] {'z8'}, dimensions={0} | all-to-all | bytes 557056 | tf_op jit(solution)/shard_map/all_to_all | solution.py:20
  34.1 1.5 %shard_map.83 = bf16[2,768,512]{2,1,0:T(8,128)(2,1)} custom-call(bf16[768,256]{1,0:T(8,128)(2,1)S(1)} %get-tuple-element.8.dispatch, bf16[8,136,128]{2,1,0:T(8,128)(2,1)S(1)} %all_to_all.25.gathered), custom_call_target="tpu_custom_call" | custom-call | tf_op jit(solution)/shard_map/pallas_call | solution.py:32
  35.6 13.4 %all-to-all-start.1 = ((bf16[64,24,512]{2,1,0:T(8,128)(2,1)}), bf16[64,24,512]{2,1,0:T(8,128)(2,1)S(1)}, u32[]{:S(2)}, u32[]{:S(2)}) async-start(bf16[64,24,512]{2,1,0:T(8,128)(2,1)} %bitcast.23), calls=%async_computation.1 | async-start | bytes 3145728 | tf_op jit(solution)/shard_map/all_to_all | solution.py:20
  49.1 2.9 %shard_map.84.down_own = bf16[4,256,512]{2,1,0:T(8,128)(2,1)} custom-call(bf16[256,2048]{1,0:T(8,128)(2,1)} %bitcast.24), custom_call_target="tpu_custom_call" | custom-call | tf_op jit(solution)/shard_map/pallas_call | solution.py:32
  52.0 2.4 %collective-permute-start.2 = (bf16[4,256,512]{2,1,0:T(8,128)(2,1)}, bf16[4,256,512]{2,1,0:T(8,128)(2,1)}, u32[]{:S(2)}, u32[]{:S(2)}) collective-permute-start(bf16[4,256,512]{2,1,0:T(8,128)(2,1)} %shard_map.84.down_own), channel_id=1, source_target_pairs={{0,1},{1,0},{2,3},{3,2},{4,5},{5,4},{6,7},{7,6},{8,9},{9,8},{10,11... | collective-permute-start | bytes 3145736 | tf_op jit(solution)/shard_map/ppermute | solution.py:24
  54.4 2.0 %collective-permute-start = (bf16[8,4,64,256]{3,2,1,0:T(8,128)(2,1)}, bf16[8,4,64,256]{3,2,1,0:T(8,128)(2,1)S(1)}, u32[]{:S(2)}, u32[]{:S(2)}) collective-permute-start(bf16[8,4,64,256]{3,2,1,0:T(8,128)(2,1)} %bitcast.5.gate_own), channel_id=1, source_target_pairs={{0,1},{1,0},{2,3},{3,2},{4,5},{5,4},{6,7},{7,6},{8,9},{9,8},{10,11... | collective-permute-start | bytes 3145736 | tf_op jit(solution)/shard_map/ppermute | solution.py:24
  56.4 2.4 %collective-permute-start.1 = (bf16[8,4,64,256]{3,2,1,0:T(8,128)(2,1)}, bf16[8,4,64,256]{3,2,1,0:T(8,128)(2,1)}, u32[]{:S(2)}, u32[]{:S(2)}) collective-permute-start(bf16[8,4,64,256]{3,2,1,0:T(8,128)(2,1)} %bitcast.6.up_own), channel_id=1, source_target_pairs={{0,1},{1,0},{2,3},{3,2},{4,5},{5,4},{6,7},{7,6},{8,9},{9,8},{10,11... | collective-permute-start | bytes 3145736 | tf_op jit(solution)/shard_map/ppermute | solution.py:24
  58.7 0.1 reshape.45
  58.8 11.0 %all-gather = f32[4,1,512]{2,1,0:T(1,128)S(1)} all-gather(f32[1,1,512]{2,1,0:T(1,128)S(1)} %reshape.45), channel_id=1, replica_groups=mesh['ep'=16,'z8'=8,'zp'=2,'core'=2] {'zp','core'}, dimensions={0}, use_global_device_ids=true | all-gather | bytes 10240 | tf_op jit(solution)/shard_map/all_gather | solution.py:274
  69.8 0.0 collective-permute-done.2.down_peer
  69.8 0.0 collective-permute-done.gate_peer
  69.8 0.0 collective-permute-done.1.up_peer
  69.8 2.1 %all-to-all-done.1 = bf16[64,24,512]{2,1,0:T(8,128)(2,1)S(1)} async-done(((bf16[64,24,512]{2,1,0:T(8,128)(2,1)}), bf16[64,24,512]{2,1,0:T(8,128)(2,1)S(1)}, u32[]{:S(2)}, u32[]{:S(2)}) %all-to-all-start.1) | async-done | bytes 1572896 | tf_op jit(solution)/shard_map/all_to_all | solution.py:20
  71.9 4.6 %shard_map.85 = bf16[4,384,512]{2,1,0:T(8,128)(2,1)S(1)} custom-call(bf16[4,384,512]{2,1,0:T(8,128)(2,1)S(1)} %bitcast.18, f32[4,512]{1,0:T(4,128)S(1)} %bitcast.21, bf16[8,4,64,256]{3,2,1,0:T(8,128)(2,1)} %bitcast.5.gate_own, bf16[8,4,64,256]{3,2,1,0:T(8,128)(2,1)} %bitcast.6.up_own, bf16[8,4,64,256]{3,2,1,0:T(8,128)(2,1)S(1)} %collective-permute-done.gate_peer, ...), custom_call_target="tpu_custom_call" | custom-call | tf_op jit(solution)/shard_map/pallas_call | solution.py:32
  76.5 0.0 copy-start
  76.5 28.0 %all_to_all.26 = bf16[64,24,512]{2,1,0:T(8,128)(2,1)S(1)} all-to-all(bf16[64,24,512]{2,1,0:T(8,128)(2,1)S(1)} %bitcast.19), channel_id=1, replica_groups=mesh['ep'=16,'z8'=8,'zp'=2,'core'=2] {'zp','core','ep'}, dimensions={0} | all-to-all | bytes 3145728 | tf_op jit(solution)/shard_map/all_to_all | solution.py:20
  104.5 0.0 copy-start.1
  104.5 0.0 copy-done
  104.5 0.6 shard_map.86
  105.1 20.1 %all_to_all.27 = bf16[8,64,256]{2,1,0:T(8,128)(2,1)S(1)} all-to-all(bf16[8,64,256]{2,1,0:T(8,128)(2,1)S(1)} %bitcast.20), channel_id=1, replica_groups=mesh['ep'=16,'z8'=8,'zp'=2,'core'=2] {'z8'}, dimensions={0} | all-to-all | bytes 524288 | tf_op jit(solution)/shard_map/all_to_all | solution.py:20
  125.3 19.5 %all_to_all.28 = f32[32,1,256]{2,1,0:T(1,128)S(1)} all-to-all(f32[32,1,256]{2,1,0:T(1,128)S(1)} %broadcast_in_dim.5), channel_id=1, replica_groups=mesh['ep'=16,'z8'=8,'zp'=2,'core'=2] {'z8','zp','core'}, dimensions={0} | all-to-all | bytes 65536 | tf_op jit(solution)/shard_map/all_to_all | solution.py:20
  144.8 0.1 reduce_sum.39
  144.9 0.0 copy-done.1
  144.9 0.7 fusion
  (6 shorter events, 0.1 us)
Async XLA Ops:
  35.6 36.3 %all-to-all-start.1 = ((bf16[64,24,512]{2,1,0:T(8,128)(2,1)}), bf16[64,24,512]{2,1,0:T(8,128)(2,1)S(1)}, u32[]{:S(2)}, u32[]{:S(2)}) async-start(bf16[64,24,512]{2,1,0:T(8,128)(2,1)} %bitcast.23), calls=%async_computation.1 | async-start | bytes 3145728 | tf_op jit(solution)/shard_map/all_to_all | solution.py:20
  52.0 17.8 %collective-permute-start.2 = (bf16[4,256,512]{2,1,0:T(8,128)(2,1)}, bf16[4,256,512]{2,1,0:T(8,128)(2,1)}, u32[]{:S(2)}, u32[]{:S(2)}) collective-permute-start(bf16[4,256,512]{2,1,0:T(8,128)(2,1)} %shard_map.84.down_own), channel_id=1, source_target_pairs={{0,1},{1,0},{2,3},{3,2},{4,5},{5,4},{6,7},{7,6},{8,9},{9,8},{10,11... | collective-permute-start | bytes 3145736 | tf_op jit(solution)/shard_map/ppermute | solution.py:24
  54.4 15.4 %collective-permute-start = (bf16[8,4,64,256]{3,2,1,0:T(8,128)(2,1)}, bf16[8,4,64,256]{3,2,1,0:T(8,128)(2,1)S(1)}, u32[]{:S(2)}, u32[]{:S(2)}) collective-permute-start(bf16[8,4,64,256]{3,2,1,0:T(8,128)(2,1)} %bitcast.5.gate_own), channel_id=1, source_target_pairs={{0,1},{1,0},{2,3},{3,2},{4,5},{5,4},{6,7},{7,6},{8,9},{9,8},{10,11... | collective-permute-start | bytes 3145736 | tf_op jit(solution)/shard_map/ppermute | solution.py:24
  56.4 13.5 %collective-permute-start.1 = (bf16[8,4,64,256]{3,2,1,0:T(8,128)(2,1)}, bf16[8,4,64,256]{3,2,1,0:T(8,128)(2,1)}, u32[]{:S(2)}, u32[]{:S(2)}) collective-permute-start(bf16[8,4,64,256]{3,2,1,0:T(8,128)(2,1)} %bitcast.6.up_own), channel_id=1, source_target_pairs={{0,1},{1,0},{2,3},{3,2},{4,5},{5,4},{6,7},{7,6},{8,9},{9,8},{10,11... | collective-permute-start | bytes 3145736 | tf_op jit(solution)/shard_map/ppermute | solution.py:24
  76.5 28.0 %copy-start = (f32[256,2]{0,1:T(2,128)S(1)}, f32[256,2]{0,1:T(2,128)}, u32[]{:S(2)}) copy-start(f32[256,2]{0,1:T(2,128)} %param.14) | copy-start | bytes 6148
  104.5 40.4 %copy-start.1 = (f32[64]{0:T(128)S(1)}, f32[64]{0:T(128)}, u32[]{:S(2)}) copy-start(f32[64]{0:T(128)} %param.15) | copy-start | bytes 772

commit v7 on v6

--- a/solution.py
+++ b/solution.py
@@ -117,9 +117,11 @@
         copy.wait()
 
 
-def reorder_kernel(down, split_down, held, turned, sems):
+def reorder_kernel(down, gate, split_down, gate_head, held, turned, sems):
     coming = pltpu.make_async_copy(down, held, sems.at[0])
     coming.start()
+    keeping = pltpu.make_async_copy(gate.at[0 : gate_head.shape[0]], gate_head, sems.at[2])
+    keeping.start()
     size = 512
     row = lax.broadcasted_iota(jnp.int32, (size, size), 0)
     col = lax.broadcasted_iota(jnp.int32, (size, size), 1)
@@ -138,28 +140,30 @@
     leaving = pltpu.make_async_copy(turned, split_down, sems.at[1])
     leaving.start()
     leaving.wait()
+    keeping.wait()
 
 
 def expert_kernel(
-    rows, gain, gate_own, up_own, gate_peer, up_peer, down_own, down_peer, sent, *scratch
+    rows, gain, head, gate_own, up_own, gate_peer, up_peer, down_own, down_peer, sent, *scratch
 ):
     held_up_peer, held_gate, held_up, down_first, down_second, scaled, sems = scratch
     parts, length, width = rows.shape
     units = gate_own.shape[-1]
+    kept = head.shape[0]
     copies = [
         pltpu.make_async_copy(source, target, sems.at[k])
         for k, (source, target) in enumerate(
             (
+                (gate_own.at[kept:], held_gate.at[kept:]),
                 (up_peer, held_up_peer),
-                (gate_own, held_gate),
                 (up_own, held_up),
                 (down_peer, down_first),
                 (down_own, down_second),
             )
         )
     ]
-    for copy in copies:
-        copy.start()
+    for k, copy in enumerate(copies):
+        copy.start(priority=k // 3)
     step = 192
     starts = range(0, length, step)
 
@@ -188,20 +192,16 @@
         mean = jnp.sum(square, axis=1, keepdims=True) / (parts * width)
         row_scale[start] = lax.rsqrt(mean + EPSILON)
         gate_pre[start] = product(start, gate_peer)
+    held_gate[0:kept] = head[...]
+    copies[0].wait()
+    own_pre = {start: product(start, held_gate) for start in starts}
     hidden = {}
-    copies[0].wait()
-    for start in starts:
-        value = gate_pre[start]
-        up_pre = product(start, held_up_peer)
-        hidden[0, start] = (value / (1.0 + jnp.exp(-value)) * up_pre).astype(BF16)
-    copies[1].wait()
-    for start in starts:
-        gate_pre[start] = product(start, held_gate)
-    copies[2].wait()
-    for start in starts:
-        value = gate_pre[start]
-        up_pre = product(start, held_up)
-        hidden[1, start] = (value / (1.0 + jnp.exp(-value)) * up_pre).astype(BF16)
+    for k, (pre, weight) in enumerate(((gate_pre, held_up_peer), (own_pre, held_up))):
+        copies[1 + k].wait()
+        for start in starts:
+            value = pre[start]
+            up_pre = product(start, weight)
+            hidden[k, start] = (value / (1.0 + jnp.exp(-value)) * up_pre).astype(BF16)
     copies[3].wait()
     copies[4].wait()
     for start in starts:
@@ -275,16 +275,20 @@
 
     gate = expert_gate.reshape(columns, 4, part_width, units)
     up = expert_up.reshape(columns, 4, part_width, units)
-    down = kernel(
+    down, gate_head = kernel(
         reorder_kernel,
-        pltpu.HBM((4, units, width), BF16),
+        [
+            pltpu.HBM((4, units, width), BF16),
+            jax.ShapeDtypeStruct((5, *gate.shape[1:]), BF16),
+        ],
         in_hbm(expert_down.reshape(units, full_width)),
-        in_specs=[HBM],
-        out_specs=HBM,
+        in_hbm(gate),
+        in_specs=[HBM] * 2,
+        out_specs=[HBM, VMEM],
         scratch_shapes=[
             pltpu.VMEM((units, full_width), BF16),
             pltpu.VMEM((4, units, width), BF16),
-            pltpu.SemaphoreType.DMA((2,)),
+            pltpu.SemaphoreType.DMA((3,)),
         ],
     )
     gate_peer = swapped(gate)
@@ -295,13 +299,14 @@
         jax.ShapeDtypeStruct((4, groups * few, width), BF16),
         rows.reshape(4, groups * few, width),
         gain,
+        gate_head,
         in_hbm(gate),
         in_hbm(up),
         gate_peer,
         in_hbm(up_peer),
         in_hbm(down),
         in_hbm(down_peer),
-        in_specs=[VMEM] * 2 + [HBM] * 2 + [VMEM] + [HBM] * 3,
+        in_specs=[VMEM] * 3 + [HBM] * 2 + [VMEM] + [HBM] * 3,
         scratch_shapes=[pltpu.VMEM(gate.shape, BF16)] * 3
         + [pltpu.VMEM(down.shape, BF16)] * 2
         + [pltpu.VMEM((groups * few, full_width), BF16), pltpu.SemaphoreType.DMA((5,))],

time: 146 us -> 146 us (level)
  transfers between devices with their start and end apart: 4 -> 4, of which waited for: 1 -> 1; matrix products, arithmetic and copies ran while one was open for 0% -> 1% of each run, Pallas kernels for 2% -> 2%
where the time goes in v7:
time: 146 us; the launch traced here: 145 us
  blocking collectives  110 us (75%)
  starting transfers between devices  20.1 us (14%)
  Pallas kernels  10.5 us (7%)
  waiting for transfers between devices  2.08 us (1%)
    all_to_all x4, blocking collectives, exchanged(): return lax.all_to_all(value, axis, split_axis=0, concat_axis=0, tiled=True)  100 us
    all_to_all x1, starting transfers between devices, exchanged(): return lax.all_to_all(value, axis, split_axis=0, concat_axis=0, tiled=True)  13.4 us
    pallas_call x5, Pallas kernels, kernel(): pl.pallas_call(body, in_specs=in_specs or [VMEM] * len(operands), out_spe...  10.5 us
    all_gather x1, blocking collectives, local(): gain = lax.all_gather(gain, ('zp', 'core'), axis=0, tiled=True)  9.75 us
    ppermute x3, starting transfers between devices, swapped(): return lax.ppermute(value, 'core', [(0, 1), (1, 0)])  6.69 us
  transfers between devices with their start and end apart: 4, of which 1 were waited for; matrix products, arithmetic and copies ran while one was open for 1% of the time, Pallas kernels for 2%

profile of v7, /device:TPU:1, one launch (start us, length us, event | category | flops | bytes accessed | tf_op | source)
XLA Modules:
  0.0 145.2 jit_solution(7897879064722960996)
XLA Ops:
  0.0 1.2 shard_map.82
  1.2 0.0 copy-start.1
  1.2 32.8 %all_to_all.25.gathered = bf16[8,136,128]{2,1,0:T(8,128)(2,1)S(1)} all-to-all(bf16[8,136,128]{2,1,0:T(8,128)(2,1)S(1)} %get-tuple-element.11), channel_id=1, replica_groups=mesh['ep'=16,'z8'=8,'zp'=2,'core'=2] {'z8'}, dimensions={0} | all-to-all | bytes 557056 | tf_op jit(solution)/shard_map/all_to_all | solution.py:20
  34.1 1.5 %shard_map.83 = bf16[2,768,512]{2,1,0:T(8,128)(2,1)} custom-call(bf16[768,256]{1,0:T(8,128)(2,1)S(1)} %get-tuple-element.10.dispatch, bf16[8,136,128]{2,1,0:T(8,128)(2,1)S(1)} %all_to_all.25.gathered), custom_call_target="tpu_custom_call" | custom-call | tf_op jit(solution)/shard_map/pallas_call | solution.py:32
  35.6 0.0 copy-done.1
  35.6 13.4 %all-to-all-start.1 = ((bf16[64,24,512]{2,1,0:T(8,128)(2,1)}), bf16[64,24,512]{2,1,0:T(8,128)(2,1)S(1)}, u32[]{:S(2)}, u32[]{:S(2)}) async-start(bf16[64,24,512]{2,1,0:T(8,128)(2,1)} %bitcast.23), calls=%async_computation.1 | async-start | bytes 3145728 | tf_op jit(solution)/shard_map/all_to_all | solution.py:20
  49.1 2.4 %collective-permute-start = (bf16[8,4,64,256]{3,2,1,0:T(8,128)(2,1)}, bf16[8,4,64,256]{3,2,1,0:T(8,128)(2,1)S(1)}, u32[]{:S(2)}, u32[]{:S(2)}) collective-permute-start(bf16[8,4,64,256]{3,2,1,0:T(8,128)(2,1)} %bitcast.24), channel_id=1, source_target_pairs={{0,1},{1,0},{2,3},{3,2},{4,5},{5,4},{6,7},{7,6},{8,9},{9,8},{10,11... | collective-permute-start | bytes 3145736 | tf_op jit(solution)/shard_map/ppermute | solution.py:24
  51.5 2.0 %collective-permute-start.1 = (bf16[8,4,64,256]{3,2,1,0:T(8,128)(2,1)}, bf16[8,4,64,256]{3,2,1,0:T(8,128)(2,1)}, u32[]{:S(2)}, u32[]{:S(2)}) collective-permute-start(bf16[8,4,64,256]{3,2,1,0:T(8,128)(2,1)} %bitcast.28), channel_id=1, source_target_pairs={{0,1},{1,0},{2,3},{3,2},{4,5},{5,4},{6,7},{7,6},{8,9},{9,8},{10,11... | collective-permute-start | bytes 3145736 | tf_op jit(solution)/shard_map/ppermute | solution.py:24
  53.4 2.9 %shard_map.84 = (bf16[4,256,512]{2,1,0:T(8,128)(2,1)}, bf16[5,4,64,256]{3,2,1,0:T(8,128)(2,1)S(1)}) custom-call(bf16[256,2048]{1,0:T(8,128)(2,1)} %bitcast.27, bf16[8,4,64,256]{3,2,1,0:T(8,128)(2,1)} %bitcast.25), custom_call_target="tpu_custom_call" | custom-call | tf_op jit(solution)/shard_map/pallas_call | solution.py:32
  56.4 2.4 %collective-permute-start.2 = (bf16[4,256,512]{2,1,0:T(8,128)(2,1)}, bf16[4,256,512]{2,1,0:T(8,128)(2,1)}, u32[]{:S(2)}, u32[]{:S(2)}) collective-permute-start(bf16[4,256,512]{2,1,0:T(8,128)(2,1)} %get-tuple-element.13.down_own), channel_id=1, source_target_pairs={{0,1},{1,0},{2,3},{3,2},{4,5},{5,4},{6,7},{7,6},{8,9},{9,8},{10,11... | collective-permute-start | bytes 3145736 | tf_op jit(solution)/shard_map/ppermute | solution.py:24
  58.7 0.6 convert_reduce_fusion.1
  59.3 0.8 reshape.45
  60.1 9.7 %all-gather = f32[4,1,512]{2,1,0:T(1,128)S(1)} all-gather(f32[1,1,512]{2,1,0:T(1,128)S(1)} %reshape.45), channel_id=1, replica_groups=mesh['ep'=16,'z8'=8,'zp'=2,'core'=2] {'zp','core'}, dimensions={0}, use_global_device_ids=true | all-gather | bytes 10240 | tf_op jit(solution)/shard_map/all_gather | solution.py:274
  69.8 0.0 collective-permute-done.gate_peer
  69.9 0.0 collective-permute-done.1.up_peer
  69.9 0.0 collective-permute-done.2.down_peer
  69.9 2.1 %all-to-all-done.1 = bf16[64,24,512]{2,1,0:T(8,128)(2,1)S(1)} async-done(((bf16[64,24,512]{2,1,0:T(8,128)(2,1)}), bf16[64,24,512]{2,1,0:T(8,128)(2,1)S(1)}, u32[]{:S(2)}, u32[]{:S(2)}) %all-to-all-start.1) | async-done | bytes 1572896 | tf_op jit(solution)/shard_map/all_to_all | solution.py:20
  71.9 4.2 %shard_map.85 = bf16[4,384,512]{2,1,0:T(8,128)(2,1)S(1)} custom-call(bf16[4,384,512]{2,1,0:T(8,128)(2,1)S(1)} %bitcast.18, f32[4,512]{1,0:T(4,128)S(1)} %bitcast.21, bf16[5,4,64,256]{3,2,1,0:T(8,128)(2,1)S(1)} %get-tuple-element.12.head, bf16[8,4,64,256]{3,2,1,0:T(8,128)(2,1)} %bitcast.26, bf16[8,4,64,256]{3,2,1,0:T(8,128)(2,1)} %bitcast.29, ...), custom_call_target="tpu_custom_call" | custom-call | tf_op jit(solution)/shard_map/pallas_call | solution.py:32
  76.2 0.0 copy-start
  76.2 0.0 copy-start.2
  76.2 28.0 %all_to_all.26 = bf16[64,24,512]{2,1,0:T(8,128)(2,1)S(1)} all-to-all(bf16[64,24,512]{2,1,0:T(8,128)(2,1)S(1)} %bitcast.19), channel_id=1, replica_groups=mesh['ep'=16,'z8'=8,'zp'=2,'core'=2] {'zp','core','ep'}, dimensions={0} | all-to-all | bytes 3145728 | tf_op jit(solution)/shard_map/all_to_all | solution.py:20
  104.2 0.0 copy-start.3
  104.2 0.0 copy-done
  104.2 0.0 copy-done.2
  104.2 0.6 shard_map.86
  104.8 20.1 %all_to_all.27 = bf16[8,64,256]{2,1,0:T(8,128)(2,1)S(1)} all-to-all(bf16[8,64,256]{2,1,0:T(8,128)(2,1)S(1)} %bitcast.20), channel_id=1, replica_groups=mesh['ep'=16,'z8'=8,'zp'=2,'core'=2] {'z8'}, dimensions={0} | all-to-all | bytes 524288 | tf_op jit(solution)/shard_map/all_to_all | solution.py:20
  125.0 19.5 %all_to_all.28 = f32[32,1,256]{2,1,0:T(1,128)S(1)} all-to-all(f32[32,1,256]{2,1,0:T(1,128)S(1)} %broadcast_in_dim.5), channel_id=1, replica_groups=mesh['ep'=16,'z8'=8,'zp'=2,'core'=2] {'z8','zp','core'}, dimensions={0} | all-to-all | bytes 65536 | tf_op jit(solution)/shard_map/all_to_all | solution.py:20
  144.4 0.1 reduce_sum.39
  144.5 0.0 copy-done.3
  144.5 0.7 fusion
  (5 shorter events, 0.1 us)
Async XLA Ops:
  1.2 34.4 %copy-start.1 = (s32[2,256]{1,0:T(2,128)}, s32[2,256]{1,0:T(2,128)S(1)}, u32[]{:S(2)}) copy-start(s32[2,256]{1,0:T(2,128)S(1)} %get-tuple-element.14.places) | copy-start | bytes 6148
  35.6 36.3 %all-to-all-start.1 = ((bf16[64,24,512]{2,1,0:T(8,128)(2,1)}), bf16[64,24,512]{2,1,0:T(8,128)(2,1)S(1)}, u32[]{:S(2)}, u32[]{:S(2)}) async-start(bf16[64,24,512]{2,1,0:T(8,128)(2,1)} %bitcast.23), calls=%async_computation.1 | async-start | bytes 3145728 | tf_op jit(solution)/shard_map/all_to_all | solution.py:20
  49.1 20.8 %collective-permute-start = (bf16[8,4,64,256]{3,2,1,0:T(8,128)(2,1)}, bf16[8,4,64,256]{3,2,1,0:T(8,128)(2,1)S(1)}, u32[]{:S(2)}, u32[]{:S(2)}) collective-permute-start(bf16[8,4,64,256]{3,2,1,0:T(8,128)(2,1)} %bitcast.24), channel_id=1, source_target_pairs={{0,1},{1,0},{2,3},{3,2},{4,5},{5,4},{6,7},{7,6},{8,9},{9,8},{10,11... | collective-permute-start | bytes 3145736 | tf_op jit(solution)/shard_map/ppermute | solution.py:24
  51.5 18.4 %collective-permute-start.1 = (bf16[8,4,64,256]{3,2,1,0:T(8,128)(2,1)}, bf16[8,4,64,256]{3,2,1,0:T(8,128)(2,1)}, u32[]{:S(2)}, u32[]{:S(2)}) collective-permute-start(bf16[8,4,64,256]{3,2,1,0:T(8,128)(2,1)} %bitcast.28), channel_id=1, source_target_pairs={{0,1},{1,0},{2,3},{3,2},{4,5},{5,4},{6,7},{7,6},{8,9},{9,8},{10,11... | collective-permute-start | bytes 3145736 | tf_op jit(solution)/shard_map/ppermute | solution.py:24
  56.4 13.5 %collective-permute-start.2 = (bf16[4,256,512]{2,1,0:T(8,128)(2,1)}, bf16[4,256,512]{2,1,0:T(8,128)(2,1)}, u32[]{:S(2)}, u32[]{:S(2)}) collective-permute-start(bf16[4,256,512]{2,1,0:T(8,128)(2,1)} %get-tuple-element.13.down_own), channel_id=1, source_target_pairs={{0,1},{1,0},{2,3},{3,2},{4,5},{5,4},{6,7},{7,6},{8,9},{9,8},{10,11... | collective-permute-start | bytes 3145736 | tf_op jit(solution)/shard_map/ppermute | solution.py:24
  76.2 28.0 %copy-start = (f32[256,2]{0,1:T(2,128)S(1)}, f32[256,2]{0,1:T(2,128)}, u32[]{:S(2)}) copy-start(f32[256,2]{0,1:T(2,128)} %param.14) | copy-start | bytes 6148
  76.2 28.0 %copy-start.2 = (s32[2,256]{1,0:T(2,128)S(1)}, s32[2,256]{1,0:T(2,128)}, u32[]{:S(2)}) copy-start(s32[2,256]{1,0:T(2,128)} %copy-done.1) | copy-start | bytes 6148
  104.2 40.4 %copy-start.3 = (f32[64]{0:T(128)S(1)}, f32[64]{0:T(128)}, u32[]{:S(2)}) copy-start(f32[64]{0:T(128)} %param.15) | copy-start | bytes 772
